TPU v7x, 32 devices: a whole 2x2x4 slice. The times are simulated.
32 devices in a mesh: fs: 8 (over z, x), tp: 4 (over y, core).
Axes of the slice: x: 2, y: 2, z: 4, core: 2. Of those that a mesh axis runs over, the one named last changes fastest.
Arguments:
- query_rows: bfloat16 [16384, 2048], P('fs', 'tp'), may hold values from -16 to 16
- key_rows: bfloat16 [16384, 2048], P('fs', 'tp'), may hold values from -8 to 8
- value_rows: bfloat16 [16384, 2048], P('fs', 'tp'), may hold values from -6 to 6
- mix_lambda: float32 [16], P('tp'), may hold values from 0.3 to 0.8
- head_gain: float32 [128], replicated, may hold values from 0.1 to 1.9
- out_cotangent: bfloat16 [16384, 2048], P('fs'), may hold values from -0.049804688 to 0.049804688
- layer_input: bfloat16 [16384, 2048], P('fs'), may hold values from -6 to 6
- value_cotangent: bfloat16 [16384, 2048], P('fs', 'tp'), may hold values from -0.049804688 to 0.049804688
- out_weight: float32 [2048, 2048], P('tp', 'fs'), may hold values from -0.125 to 0.125
- value_weight: float32 [2048, 2048], P('fs', 'tp'), may hold values from -0.125 to 0.125
- out_basis: bfloat16 [2048, 256], replicated, may hold values from -0.125 to 0.125
- value_basis: bfloat16 [2048, 256], replicated, may hold values from -0.125 to 0.125
- out_first: float32 [256, 2048], P('fs', 'tp'), may hold values from -20 to 20
- out_second: float32 [256, 2048], P('fs', 'tp'), may hold values from 0.02 to 0.5
- value_first: float32 [256, 2048], P('fs', 'tp'), may hold values from -20 to 20
- value_second: float32 [256, 2048], P('fs', 'tp'), may hold values from 0.02 to 0.5
Outputs:
- out_step: float32 [2048, 2048], P('tp', 'fs')
- value_step: float32 [2048, 2048], P('fs', 'tp')
- new_out_weight: float32 [2048, 2048], P('tp', 'fs')
- new_value_weight: float32 [2048, 2048], P('fs', 'tp')
- out_copy: bfloat16 [2048, 2048], P('tp')
- value_copy: bfloat16 [2048, 2048], P(None, 'tp')
- new_out_first: float32 [256, 2048], P('fs', 'tp')
- new_out_second: float32 [256, 2048], P('fs', 'tp')
- new_value_first: float32 [256, 2048], P('fs', 'tp')
- new_value_second: float32 [256, 2048], P('fs', 'tp')
All inputs are finite; a program needn't handle non-finite values.
Results may differ from a plain program's by a relative error of at most 0.001.
Values may be sent and summed in bfloat16 or wider, within the bound.
No kernel may reach another device: no remote copies, remote signals or barrier semaphores. Data moves between devices by JAX's collectives and lax.ppermute only.
A program may use at most 192 MiB of HBM per device.

v0:
```python
import functools
import math

import jax
import jax.numpy as jnp
from jax import lax
from jax.experimental import pallas as pl
from jax.experimental.pallas import tpu as pltpu
from jax.sharding import PartitionSpec as P

DV = 128

EPSILON_NORM = 1e-05
EPSILON_ADAM = 1e-08
BETA_ONE = 0.9
BETA_TWO = 0.95
CLIP_RMS = 1.0
LEARN_RATE = 0.01
LOG2E = math.log2(math.e)

F32 = jnp.float32
BF16 = jnp.bfloat16
NT = (((1,), (1,)), ((), ()))
VMEM_BYTES = 60 * 2**20


def split_pair(x):
    high = x.astype(BF16)
    return high, (x - high.astype(F32)).astype(BF16)


def value_proj_kernel(x_ref, c_ref, basis_ref, proj_ref):
    y = jnp.dot(x_ref[...], basis_ref[...], preferred_element_type=F32)
    high, low = split_pair(y.T)
    part = jnp.dot(high, c_ref[...], preferred_element_type=F32) + jnp.dot(
        low, c_ref[...], preferred_element_type=F32
    )

    @pl.when(pl.program_id(0) == 0)
    def _():
        proj_ref[...] = part

    @pl.when(pl.program_id(0) > 0)
    def _():
        proj_ref[...] += part


def value_proj(x, c, basis):
    tokens, width = x.shape
    rank, cols = basis.shape[1], c.shape[1]
    block = min(512, tokens)
    return pl.pallas_call(
        value_proj_kernel,
        grid=(tokens // block,),
        out_shape=jax.ShapeDtypeStruct((rank, cols), F32),
        in_specs=[
            pl.BlockSpec((block, width), lambda t: (t, 0)),
            pl.BlockSpec((block, cols), lambda t: (t, 0)),
            pl.BlockSpec((width, rank), lambda t: (0, 0)),
        ],
        out_specs=pl.BlockSpec((rank, cols), lambda t: (0, 0)),
        cost_estimate=pl.CostEstimate(
            flops=2 * tokens * rank * (width + 2 * cols),
            bytes_accessed=2 * tokens * (width + cols),
            transcendentals=0,
        ),
        compiler_params=pltpu.CompilerParams(vmem_limit_bytes=VMEM_BYTES),
        name="value_proj",
    )(x, c, basis)


def low_rank_kernel(x_ref, basis_ref, high_ref, low_ref):
    y = jnp.dot(x_ref[...], basis_ref[...], preferred_element_type=F32)
    high, low = split_pair(y.T)
    high_ref[...] = high
    low_ref[...] = low


def low_rank_rows(half, x, basis):
    tokens, width = x.shape[0] // 2, x.shape[1]
    rank = basis.shape[1]
    block = min(512, tokens)
    skip = half * (tokens // block)
    out = jax.ShapeDtypeStruct((rank, tokens), BF16)
    return pl.pallas_call(
        low_rank_kernel,
        grid=(tokens // block,),
        out_shape=(out, out),
        in_specs=[
            pl.BlockSpec((block, width), lambda t: (t + skip, 0)),
            pl.BlockSpec((width, rank), lambda t: (0, 0)),
        ],
        out_specs=[pl.BlockSpec((rank, block), lambda t: (0, t))] * 2,
        cost_estimate=pl.CostEstimate(
            flops=2 * tokens * rank * width,
            bytes_accessed=2 * tokens * width,
            transcendentals=0,
        ),
        compiler_params=pltpu.CompilerParams(vmem_limit_bytes=VMEM_BYTES),
        name="low_rank_rows",
    )(x, basis)


def attend_kernel(
    bq, start, lam_ref, gain_ref, q_hbm, k_hbm, v_hbm, high_hbm, low_hbm, high_two,
    low_two, *rest
):
    proj_ref, q_all, k_all, v_all, high_ref, low_ref, e_ref, h_ref, sum_ref, sems, late_sems = (
        rest[-11:]
    )
    count, seq, width = q_all.shape
    step = pl.program_id(0)

    def head_copies(j):
        columns = pl.ds(pl.multiple_of((start + j) * width, width), width)
        return [
            pltpu.make_async_copy(source.at[:, columns], target.at[j], sems.at[j, i])
            for i, (source, target) in enumerate(
                ((k_hbm, k_all), (q_hbm, q_all), (v_hbm, v_all))
            )
        ]

    def late_copies():
        pairs = ((high_hbm, high_ref), (low_hbm, low_ref), (high_two, high_ref), (low_two, low_ref))
        return [
            pltpu.make_async_copy(
                source,
                target.at[:, pl.ds(i // 2 * (seq // 2), seq // 2)],
                late_sems.at[i],
            )
            for i, (source, target) in enumerate(pairs)
        ]

    @pl.when(step == 0)
    def _():
        for copy in head_copies(0):
            copy.start()
        for copy in late_copies():
            copy.start()
        for j in range(1, count):
            for copy in head_copies(j):
                copy.start()

    for copy in head_copies(step):
        copy.wait()
    q_ref, k_ref, v_ref = q_all.at[step], k_all.at[step], v_all.at[step]
    half = width // 2
    lam = lam_ref[start + step]
    scale = half**-0.5
    first = lax.broadcasted_iota(jnp.int32, (1, width), 1) < half

    mark = (
        lax.broadcasted_iota(jnp.int32, (width, 128), 0) // half
        == lax.broadcasted_iota(jnp.int32, (width, 128), 1) // 64
    ).astype(BF16)

    def top_norm(ref):
        x = ref[...]
        return jnp.max(
            jnp.dot(x * x, mark, preferred_element_type=F32), axis=0, keepdims=True
        )

    bound = jnp.max(top_norm(q_ref) * top_norm(k_ref))
    small = bound < (70.0 / scale) ** 2

    def finish(base, rows, mix, values):
        raw = jnp.dot(mix, values, preferred_element_type=F32)
        square = jnp.mean(raw * raw, axis=-1, keepdims=True)
        normed = raw * lax.rsqrt(square + EPSILON_NORM) * gain_ref[...]
        h_ref[pl.ds(base, rows), :] = normed.astype(BF16)

    @pl.when(small)
    def _():
        keep = lax.broadcasted_iota(jnp.int32, (bq, bq), 1) <= lax.broadcasted_iota(
            jnp.int32, (bq, bq), 0
        )
        keep_both = jnp.concatenate([keep, keep], axis=0)
        for i in range(seq // bq):
            slot = i % 2
            q = q_ref[i * bq : (i + 1) * bq, :]
            zero = jnp.zeros_like(q)
            both = jnp.concatenate(
                [jnp.where(first, q, zero), jnp.where(first, zero, q)], axis=0
            )
            for t in range(i + 1):
                scores = lax.dot_general(
                    both, k_ref[t * bq : (t + 1) * bq, :], NT, preferred_element_type=F32
                )
                e = jnp.exp2(scores * (scale * LOG2E))
                if t == i:
                    e = jnp.where(keep_both, e, 0.0)
                e_ref[slot, :, t * bq : (t + 1) * bq] = e
                part = e[:, :128]
                for c in range(1, bq // 128):
                    part = part + e[:, c * 128 : (c + 1) * 128]
                if t == 0:
                    sum_ref[slot] = part
                else:
                    sum_ref[slot] += part
            total = jnp.sum(sum_ref[slot], axis=-1, keepdims=True)
            one = 1.0 / total[:bq]
            two = lam / total[bq:]
            n = (i + 1) * bq
            mix = e_ref[slot, :bq, :n] * one - e_ref[slot, bq:, :n] * two
            finish(i * bq, bq, mix.astype(BF16), v_ref[:n, :])

    @pl.when(jnp.logical_not(small))
    def _():
        few = min(64, bq)

        def block(i, carry):
            base = pl.multiple_of(i * few, few)
            q = q_ref[pl.ds(base, few), :]
            zero = jnp.zeros_like(q)
            both = jnp.concatenate(
                [jnp.where(first, q, zero), jnp.where(first, zero, q)], axis=0
            )
            scores = (
                lax.dot_general(both, k_ref[...], NT, preferred_element_type=F32) * scale
            )
            row = lax.broadcasted_iota(jnp.int32, (few, seq), 0)
            keep = lax.broadcasted_iota(jnp.int32, (few, seq), 1) <= base + row
            scores = jnp.where(jnp.concatenate([keep, keep], axis=0), scores, -jnp.inf)
            e_ref[0, : 2 * few, :] = jnp.exp(
                scores - jnp.max(scores, axis=-1, keepdims=True)
            )
            total = jnp.sum(e_ref[0, : 2 * few, :], axis=-1, keepdims=True)
            mix = e_ref[0, :few, :] * (1.0 / total[:few]) - e_ref[0, few : 2 * few, :] * (
                lam / total[few:]
            )
            finish(base, few, mix.astype(BF16), v_ref[...])
            return carry

        lax.fori_loop(0, seq // few, block, 0)

    @pl.when(step == 0)
    def _():
        for copy in late_copies():
            copy.wait()

    h = h_ref[...]
    proj_ref[...] = jnp.dot(high_ref[...], h, preferred_element_type=F32) + jnp.dot(
        low_ref[...], h, preferred_element_type=F32
    )


def attend_heads(start, stop, query_rows, key_rows, value_rows, mix_lambda, head_gain, pairs, prev):
    seq = query_rows.shape[0]
    heads = mix_lambda.shape[0]
    count = stop - start
    width = query_rows.shape[1] // heads
    rank = pairs[0][0].shape[0]
    bq = min(256, seq)
    hbm = pl.BlockSpec(memory_space=pl.ANY)
    earlier = () if prev is None else (prev,)
    return pl.pallas_call(
        functools.partial(attend_kernel, bq, start),
        grid=(count,),
        out_shape=jax.ShapeDtypeStruct((rank, heads * DV), F32),
        in_specs=[
            pl.BlockSpec(memory_space=pltpu.SMEM),
            pl.BlockSpec(memory_space=pltpu.VMEM),
        ]
        + [hbm] * (7 + len(earlier)),
        out_specs=pl.BlockSpec((rank, DV), lambda j: (0, j + start)),
        input_output_aliases={9: 0} if earlier else {},
        scratch_shapes=[
            pltpu.VMEM((count, seq, width), BF16),
            pltpu.VMEM((count, seq, width), BF16),
            pltpu.VMEM((count, seq, DV), BF16),
            pltpu.VMEM((rank, seq), BF16),
            pltpu.VMEM((rank, seq), BF16),
            pltpu.VMEM((2, 2 * bq, seq), F32),
            pltpu.VMEM((seq, DV), BF16),
            pltpu.VMEM((2, 2 * bq, 128), F32),
            pltpu.SemaphoreType.DMA((count, 3)),
            pltpu.SemaphoreType.DMA((4,)),
        ],
        cost_estimate=pl.CostEstimate(
            flops=8 * count * seq * seq * DV,
            bytes_accessed=2 * seq * (count * (2 * width + DV) + 2 * rank),
            transcendentals=count * seq * seq,
        ),
        compiler_params=pltpu.CompilerParams(vmem_limit_bytes=VMEM_BYTES),
        name="attend_heads",
    )(
        mix_lambda,
        head_gain.reshape(1, DV),
        query_rows,
        key_rows,
        value_rows,
        *pairs[0],
        *pairs[1],
        *earlier,
    )


def out_final_kernel(entries, owner_ref, sum_ref, rank_owner_ref, basis_ref, *refs):
    parts, refs = refs[:4], refs[4:]
    direction, (copy_ref, step_ref, weight_ref, dir_ref, total_ref, held_ref, sems) = (
        refs[:-7], refs[-7:],
    )
    half, rows, share = parts[0].shape
    copies = []
    for p, part in enumerate(parts):
        copy = pltpu.make_async_copy(part, held_ref.at[pl.ds(p * half, half)], sems.at[p])
        copy.start()
        copies.append(copy)
    place_rows(rank_owner_ref, direction, dir_ref)
    high, low = split_pair(dir_ref[...].T)
    total_ref[...] = clip_of(sum_ref, entries) * (
        lax.dot_general(high, basis_ref[...], NT, preferred_element_type=F32)
        + lax.dot_general(low, basis_ref[...], NT, preferred_element_type=F32)
    )
    for p, copy in enumerate(copies):
        copy.wait()
        at = pl.ds((p // 2) * rows, rows)

        def one(a, carry):
            slot = p * half + a
            columns = pl.ds(pl.multiple_of(owner_ref[slot] * share, share), share)
            weight = held_ref[slot] - LEARN_RATE * total_ref[at, columns]
            copy_ref[at, columns] = weight.astype(BF16)
            return carry

        lax.fori_loop(0, half, one, 0)
    own = pl.ds(pl.multiple_of(owner_ref[0] * share, share), share)
    for g in range(2):
        at = pl.ds(g * rows, rows)
        step = total_ref[at, own]
        step_ref[at, :] = step
        weight_ref[at, :] = held_ref[2 * g * half] - LEARN_RATE * step


def out_final(owners, squares, entries, rank_owners, direction, basis, parts):
    half, rows, share = parts[0].shape
    width, rank = basis.shape
    cols = 2 * rows
    smem = pl.BlockSpec(memory_space=pltpu.SMEM)
    vmem = pl.BlockSpec(memory_space=pltpu.VMEM)
    block = jax.ShapeDtypeStruct((cols, share), F32)
    return pl.pallas_call(
        functools.partial(out_final_kernel, entries),
        out_shape=(jax.ShapeDtypeStruct((cols, width), BF16), block, block),
        in_specs=[smem, vmem, smem, vmem]
        + [pl.BlockSpec(memory_space=pl.ANY)] * 4
        + [vmem] * len(direction),
        out_specs=[vmem] * 3,
        scratch_shapes=[
            pltpu.VMEM((rank, cols), F32),
            pltpu.VMEM((cols, width), F32),
            pltpu.VMEM((4 * half, rows, share), F32),
            pltpu.SemaphoreType.DMA((4,)),
        ],
        cost_estimate=pl.CostEstimate(
            flops=4 * rank * cols * width,
            bytes_accessed=6 * cols * width,
            transcendentals=0,
        ),
        compiler_params=pltpu.CompilerParams(vmem_limit_bytes=VMEM_BYTES),
        name="out_final",
    )(owners, squares, rank_owners, basis, *parts, *direction)


def place_rows(owner_ref, parts, out_ref):
    blocks = owner_ref.shape[0] // len(parts)
    rows = parts[0].shape[0] // blocks
    for p, part in enumerate(parts):
        for a in range(blocks):
            at = pl.multiple_of(owner_ref[p * blocks + a] * rows, rows)
            out_ref[pl.ds(at, rows), :] = part[a * rows : (a + 1) * rows, :]


def clip_of(total_ref, entries):
    total = jnp.sum(
        jnp.sum(total_ref[...], axis=0, keepdims=True), axis=1, keepdims=True
    )
    return jnp.minimum(1.0, CLIP_RMS * math.sqrt(entries) / jnp.sqrt(total))


def value_final_kernel(
    entries, me_ref, sum_ref, owner_ref, basis_ref, old_ref, *refs
):
    parts, (step_ref, weight_ref, copy_ref, dir_ref) = refs[:-4], refs[-4:]
    place_rows(owner_ref, parts, dir_ref)
    high, low = split_pair(dir_ref[...])
    total = jnp.dot(basis_ref[...], high, preferred_element_type=F32) + jnp.dot(
        basis_ref[...], low, preferred_element_type=F32
    )
    step = clip_of(sum_ref, entries) * total
    weight = old_ref[...] - LEARN_RATE * step
    step_ref[...] = step
    weight_ref[...] = weight
    copy_ref[...] = weight.astype(BF16)


def value_final(me, squares, entries, owners, direction, basis, old):
    rows, cols = old.shape
    rank = basis.shape[1]
    block = jax.ShapeDtypeStruct((rows, cols), F32)
    whole = lambda shape: pl.BlockSpec(shape, lambda i, me: (0, 0))
    smem = pl.BlockSpec(memory_space=pltpu.SMEM)
    grid_spec = pltpu.PrefetchScalarGridSpec(
        num_scalar_prefetch=1,
        grid=(1,),
        in_specs=[
            whole(squares.shape),
            smem,
            pl.BlockSpec((rows, rank), lambda i, me: (me[0], 0)),
            whole((rows, cols)),
        ]
        + [whole(part.shape) for part in direction],
        out_specs=[whole((rows, cols))] * 3,
        scratch_shapes=[pltpu.VMEM((rank, cols), F32)],
    )
    return pl.pallas_call(
        functools.partial(value_final_kernel, entries),
        grid_spec=grid_spec,
        out_shape=(block, block, jax.ShapeDtypeStruct((rows, cols), BF16)),
        cost_estimate=pl.CostEstimate(
            flops=4 * rank * cols * rows,
            bytes_accessed=14 * old.size,
            transcendentals=0,
        ),
        name="value_final",
    )(me.reshape(1), squares, owners, basis, old, *direction)


def fold(part, arrived, inner, width, outer, groups, rows):
    cols = part.shape[1]
    vmem = pl.BlockSpec(memory_space=pltpu.VMEM)
    place = jnp.stack([inner, jnp.int32(width), outer]).astype(jnp.int32)
    return pl.pallas_call(
        functools.partial(fold_kernel, len(arrived)),
        out_shape=[jax.ShapeDtypeStruct((rows, cols), F32)] * groups,
        in_specs=[pl.BlockSpec(memory_space=pltpu.SMEM)] + [vmem] * (1 + len(arrived)),
        out_specs=[vmem] * groups,
        cost_estimate=pl.CostEstimate(
            flops=part.size, bytes_accessed=8 * part.size, transcendentals=0
        ),
        name="fold",
    )(place, part, *arrived)


def fold_kernel(count, place_ref, part_ref, *refs):
    arrived, outs = refs[:count], refs[count:]
    rows = outs[0].shape[0]
    for d, out in enumerate(outs):
        member = place_ref[2] ^ d
        at = pl.multiple_of((member * place_ref[1] + place_ref[0]) * rows, rows)
        total = part_ref[pl.ds(at, rows), :]
        for other in arrived:
            total = total + other[pl.ds(pl.multiple_of(member * rows, rows), rows), :]
        out[...] = total


def square_kernel(*refs):
    parts, out_ref = refs[:-1], refs[-1]
    sums = []
    for part in parts:
        rows, cols = part.shape
        total = jnp.zeros((8, 128), F32)
        for r in range(rows // 8):
            for c in range(cols // 128):
                x = part[r * 8 : (r + 1) * 8, c * 128 : (c + 1) * 128]
                total = total + x * x
        sums.append(total)
    while len(sums) > 1:
        sums = [a + b for a, b in zip(sums[::2], sums[1::2])]
    out_ref[...] = sums[0]


def square_sums(parts):
    vmem = pl.BlockSpec(memory_space=pltpu.VMEM)
    return pl.pallas_call(
        square_kernel,
        out_shape=jax.ShapeDtypeStruct((8, 128), F32),
        in_specs=[vmem] * len(parts),
        out_specs=vmem,
        cost_estimate=pl.CostEstimate(
            flops=2 * len(parts) * parts[0].size,
            bytes_accessed=4 * len(parts) * parts[0].size,
            transcendentals=0,
        ),
        name="square_sums",
    )(*parts)


def assemble_kernel(owner_ref, *refs):
    parts, out_ref = refs[:4], refs[4]
    half, rows, _ = parts[0].shape
    for p, part in enumerate(parts):
        def one(a, carry):
            at = pl.multiple_of(owner_ref[p * half + a] * (2 * rows) + (p // 2) * rows, rows)
            out_ref[pl.ds(at, rows), :] = part[a]
            return carry

        lax.fori_loop(0, half, one, 0)


def assemble(owners, parts):
    half, rows, cols = parts[0].shape
    vmem = pl.BlockSpec(memory_space=pltpu.VMEM)
    return pl.pallas_call(
        assemble_kernel,
        out_shape=jax.ShapeDtypeStruct((4 * half * rows, cols), parts[0].dtype),
        in_specs=[pl.BlockSpec(memory_space=pltpu.SMEM)] + [vmem] * 4,
        out_specs=vmem,
        cost_estimate=pl.CostEstimate(
            flops=0, bytes_accessed=16 * half * rows * cols, transcendentals=0
        ),
        compiler_params=pltpu.CompilerParams(vmem_limit_bytes=VMEM_BYTES),
        name="assemble",
    )(owners, *parts)


def swap(x, axis, bit):
    n = lax.axis_size(axis)
    return lax.ppermute(x, axis, [(i, i ^ bit) for i in range(n)])


def bits_down(n):
    bits = [1 << b for b in range(n.bit_length() - 1)]
    return bits[::-1]


def groups_of(axis):
    n = lax.axis_size(axis)
    outer = min(4, n)
    return outer, n // outer


def reduce_scatter(x, axis):
    outer, inner = groups_of(axis)
    me = lax.axis_index(axis)
    rows, cols = x.shape[0] // (outer * inner), x.shape[1]
    place_out, place_in = me // inner, me % inner
    blocks = x.reshape(outer, inner, rows, cols)
    arrived = []
    for d in range(1, inner):
        send = lax.dynamic_index_in_dim(blocks, place_in ^ d, 1, keepdims=False)
        arrived.append(swap(send.reshape(outer * rows, cols), axis, d))
    sums = fold(x, arrived, place_in, inner, place_out, outer, rows)
    total = sums[0]
    for d in range(1, outer):
        total = total + swap(sums[d], axis, d * inner)
    return total


def gather_and_square(x):
    axis = "fs"
    outer, inner = groups_of(axis)
    near = [x] + [swap(x, axis, d * inner) for d in range(1, outer)]
    squares = square_sums(near)
    near = jnp.concatenate(near, axis=0)
    parts = [near] + [swap(near, axis, d) for d in range(1, inner)]
    away = [p ^ (d * inner) for p in range(inner) for d in range(outer)]
    owners = jnp.array(away, jnp.int32) ^ lax.axis_index(axis)
    squares = sum_over(squares, "tp", lax.axis_size("tp"))
    squares = sum_over(squares, axis, inner)
    return parts, owners, squares, x.size * lax.axis_size(axis) * lax.axis_size("tp")


def gather_by_distance(x, axis):
    bits = bits_down(lax.axis_size(axis))
    other = swap(x, axis, bits[0])
    rows = x.shape[0] // 2
    parts, owners = [], []
    for g, order in enumerate((bits[:0:-1], bits[1:])):
        cut = slice(g * rows, (g + 1) * rows)
        piece = jnp.stack([x[cut], other[cut]])
        away = [0, bits[0]]
        for bit in order[:-1]:
            piece = jnp.concatenate([piece, swap(piece, axis, bit)])
            away = away + [a ^ bit for a in away]
        last = order[-1]
        parts += [piece, swap(piece, axis, last)]
        owners += away + [a ^ last for a in away]
    return parts, jnp.array(owners, jnp.int32) ^ lax.axis_index(axis)


def sum_over(x, axis, group):
    for bit in bits_down(group)[::-1]:
        x = x + swap(x, axis, bit)
    return x


def moment_step(proj, first, second):
    new_first = BETA_ONE * first + (1.0 - BETA_ONE) * proj
    new_second = BETA_TWO * second + (1.0 - BETA_TWO) * proj * proj
    direction = new_first / (jnp.sqrt(new_second) + EPSILON_ADAM)
    return (new_first, new_second, direction)


def body(
    query_rows,
    key_rows,
    value_rows,
    mix_lambda,
    head_gain,
    out_cotangent,
    layer_input,
    value_cotangent,
    out_weight,
    value_weight,
    out_basis,
    value_basis,
    out_first,
    out_second,
    value_first,
    value_second,
):
    me = lax.axis_index("fs")
    parts, owners = gather_by_distance(out_weight, "fs")

    value_part = value_proj(layer_input, value_cotangent, value_basis)
    value_sum = reduce_scatter(value_part, "fs")
    new_value_first, new_value_second, value_dir = moment_step(
        value_sum, value_first, value_second
    )
    value_dirs, value_owners, *value_squares = gather_and_square(value_dir)
    value_step, new_value_weight, value_rounded = value_final(
        me, *value_squares, value_owners, value_dirs, value_basis, value_weight
    )
    value_copy = assemble(owners, gather_by_distance(value_rounded, "fs")[0])

    pairs = [low_rank_rows(half, out_cotangent, out_basis) for half in range(2)]
    heads = mix_lambda.shape[0]
    out_part = None
    cuts = sorted({0, heads // 4, heads // 2, heads})
    for start, stop in zip(cuts[:-1], cuts[1:]):
        out_part = attend_heads(
            start, stop, query_rows, key_rows,
            value_rows, mix_lambda, head_gain, pairs, out_part,
        )
    out_sum = reduce_scatter(out_part, "fs")
    new_out_first, new_out_second, out_dir = moment_step(out_sum, out_first, out_second)
    out_dirs, out_owners, *out_squares = gather_and_square(out_dir)
    out_copy, out_step, new_out_weight = out_final(
        owners, *out_squares, out_owners, out_dirs, out_basis, parts
    )
    return (
        out_step,
        value_step,
        new_out_weight,
        new_value_weight,
        out_copy,
        value_copy,
        new_out_first,
        new_out_second,
        new_value_first,
        new_value_second,
    )


def solution(mesh):
    split, rows = P("fs", "tp"), P("fs", None)
    placed = (
        split, split, split, P("tp"), P(), rows, rows, split,
        P("tp", "fs"), split, P(), P(), split, split, split, split,
    )
    return jax.shard_map(
        body,
        mesh=mesh,
        in_specs=placed,
        out_specs=(
            P("tp", "fs"), split, P("tp", "fs"), split, P("tp", None), P(None, "tp"),
            split, split, split, split,
        ),
        check_vma=False,
    )
```

profile of v0, /device:TPU:0, one launch (start us, length us, event | category | flops | bytes accessed | tf_op | source)
XLA Modules:
  0.0 298.8 jit_solution(738630002397220782)
XLA Ops:
  0.7 9.4 %value_proj.1.part_ref = f32[256,512]{1,0:T(8,128)} custom-call(bf16[2048,2048]{1,0:T(8,128)(2,1)} %x_ref.5, bf16[2048,512]{1,0:T(8,128)(2,1)} %c_ref.1, bf16[2048,256]{1,0:T(8,128)(2,1)} %basis_ref.9), custom_call_target="tpu_custom_call" | custom-call | flops 3221225472 | bytes 10485760 | tf_op jit(solution)/shard_map/value_proj/pallas_call | solution.py:52
  11.1 3.0 %collective-permute-start.16 = (f32[128,512]{1,0:T(8,128)S(1)}, f32[128,512]{1,0:T(8,128)S(1)}, u32[]{:S(2)}, u32[]{:S(2)}) collective-permute-start(f32[128,512]{1,0:T(8,128)S(1)} %bitcast.30), channel_id=1, source_target_pairs={{0,4},{4,0},{8,12},{12,8},{16,20},{20,16},{24,28},{28,24},{1,5},{5... | collective-permute-start | bytes 786440 | tf_op jit(solution)/shard_map/ppermute | solution.py:519
  14.1 4.2 %low_rank_rows.2 = (bf16[256,1024]{1,0:T(8,128)(2,1)}, bf16[256,1024]{1,0:T(8,128)(2,1)}) custom-call(bf16[2048,2048]{1,0:T(8,128)(2,1)} %x_ref.4, bf16[2048,256]{1,0:T(8,128)(2,1)} %basis_ref.7), custom_call_target="tpu_custom_call" | custom-call | flops 1073741824 | bytes 4194304 | tf_op jit(solution)/shard_map/low_rank_rows/pallas_call | solution.py:85
  18.3 4.2 %low_rank_rows.3 = (bf16[256,1024]{1,0:T(8,128)(2,1)}, bf16[256,1024]{1,0:T(8,128)(2,1)}) custom-call(bf16[2048,2048]{1,0:T(8,128)(2,1)} %x_ref.4, bf16[2048,256]{1,0:T(8,128)(2,1)} %basis_ref.7), custom_call_target="tpu_custom_call" | custom-call | flops 1073741824 | bytes 4194304 | tf_op jit(solution)/shard_map/low_rank_rows/pallas_call | solution.py:85
  23.2 33.6 %attend_heads.3.rest_0_ = f32[256,512]{1,0:T(8,128)} custom-call(f32[4]{0:T(128)} %lam_ref.5, f32[1,128]{1,0:T(1,128)} %bitcast.32, bf16[2048,512]{1,0:T(8,128)(2,1)} %q_hbm.5, bf16[2048,512]{1,0:T(8,128)(2,1)} %k_hbm.5, bf16[2048,512]{1,0:T(8,128)(2,1)} %v_hbm.5, bf16[256,1024]{1,0:T(8,128)(2,1)} %get-tuple-element.28.high_hbm, ...), custom_call_target="tpu_custom_call" | custom-call | flops 4294967296 | bytes 3670016 | tf_op jit(solution)/shard_map/attend_heads/pallas_call | solution.py:256
  56.8 33.8 %attend_heads.4.rest_0_ = f32[256,512]{1,0:T(8,128)} custom-call(f32[4]{0:T(128)} %lam_ref.5, f32[1,128]{1,0:T(1,128)} %bitcast.33, bf16[2048,512]{1,0:T(8,128)(2,1)} %q_hbm.5, bf16[2048,512]{1,0:T(8,128)(2,1)} %k_hbm.5, bf16[2048,512]{1,0:T(8,128)(2,1)} %v_hbm.5, bf16[256,1024]{1,0:T(8,128)(2,1)} %get-tuple-element.28.high_hbm, ...), custom_call_target="tpu_custom_call", output_to_operand_aliasing={{}: (9, {})} | custom-call | flops 4294967296 | bytes 3670016 | tf_op jit(solution)/shard_map/attend_heads/pallas_call | solution.py:256
  93.1 3.6 %collective-permute-start.19 = (f32[32,512]{1,0:T(8,128)}, f32[32,512]{1,0:T(8,128)S(1)}, u32[]{:S(2)}, u32[]{:S(2)}) collective-permute-start(f32[32,512]{1,0:T(8,128)} %get-tuple-element.40), channel_id=1, source_target_pairs={{0,24},{4,28},{8,16},{12,20},{16,8},{20,12},{24,0},{28,4},{1,25},{... | collective-permute-start | bytes 196616 | tf_op jit(solution)/shard_map/ppermute | solution.py:519
  97.6 63.6 %attend_heads.5.part_ref = f32[256,512]{1,0:T(8,128)} custom-call(f32[4]{0:T(128)} %lam_ref.5, f32[1,128]{1,0:T(1,128)} %bitcast.34, bf16[2048,512]{1,0:T(8,128)(2,1)} %q_hbm.5, bf16[2048,512]{1,0:T(8,128)(2,1)} %k_hbm.5, bf16[2048,512]{1,0:T(8,128)(2,1)} %v_hbm.5, bf16[256,1024]{1,0:T(8,128)(2,1)} %get-tuple-element.28.high_hbm, ...), custom_call_target="tpu_custom_call", output_to_operand_aliasing={{}: (9, {})} | custom-call | flops 8589934592 | bytes 5242880 | tf_op jit(solution)/shard_map/attend_heads/pallas_call | solution.py:256
  163.2 2.9 collective-permute-start.21
  169.4 12.5 %collective-permute-done.21.refs_2_ = f32[32,512]{1,0:T(8,128)S(1)} collective-permute-done((f32[32,512]{1,0:T(8,128)S(1)}, f32[32,512]{1,0:T(8,128)S(1)}, u32[]{:S(2)}, u32[]{:S(2)}) %collective-permute-start.21) | collective-permute-done | bytes 65568 | tf_op jit(solution)/shard_map/ppermute | solution.py:519
  191.3 2.3 collective-permute-start.3
  195.1 2.1 collective-permute-start.26
  198.6 5.8 %collective-permute-done.26.refs_1_ = f32[128,512]{1,0:T(8,128)S(1)} collective-permute-done((f32[128,512]{1,0:T(8,128)S(1)}, f32[128,512]{1,0:T(8,128)S(1)}, u32[]{:S(2)}, u32[]{:S(2)}) %collective-permute-start.26) | collective-permute-done | bytes 262176 | tf_op jit(solution)/shard_map/ppermute | solution.py:519
  205.1 2.7 value_final.1
  207.8 2.4 collective-permute-start.27
  212.3 7.4 %collective-permute-done.27 = bf16[256,512]{1,0:T(8,128)(2,1)S(1)} collective-permute-done((bf16[256,512]{1,0:T(8,128)(2,1)}, bf16[256,512]{1,0:T(8,128)(2,1)S(1)}, u32[]{:S(2)}, u32[]{:S(2)}) %collective-permute-start.27) | collective-permute-done | bytes 262176 | tf_op jit(solution)/shard_map/ppermute | solution.py:519
  221.9 5.1 %collective-permute-done.13 = f32[2,256,256]{2,1,0:T(8,128)S(1)} collective-permute-done((f32[2,256,256]{2,1,0:T(8,128)S(1)}, f32[2,256,256]{2,1,0:T(8,128)S(1)}, u32[]{:S(2)}, u32[]{:S(2)}) %collective-permute-start.13) | collective-permute-done | bytes 524320 | tf_op jit(solution)/shard_map/ppermute | solution.py:519
  227.1 2.5 collective-permute-start.12
  234.4 25.5 %collective-permute-done.30 = bf16[2,128,512]{2,1,0:T(8,128)(2,1)S(1)} collective-permute-done((bf16[2,128,512]{2,1,0:T(8,128)(2,1)S(1)}, bf16[2,128,512]{2,1,0:T(8,128)(2,1)S(1)}, u32[]{:S(2)}, u32[]{:S(2)}) %collective-permute-start.30) | collective-permute-done | bytes 262176 | tf_op jit(solution)/shard_map/ppermute | solution.py:519
  262.1 6.5 %collective-permute-done.5.refs_2_ = f32[32,512]{1,0:T(8,128)S(1)} collective-permute-done((f32[32,512]{1,0:T(8,128)S(1)}, f32[32,512]{1,0:T(8,128)S(1)}, u32[]{:S(2)}, u32[]{:S(2)}) %collective-permute-start.5) | collective-permute-done | bytes 65568 | tf_op jit(solution)/shard_map/ppermute | solution.py:519
  270.1 4.6 %collective-permute-done.6.refs_3_ = f32[32,512]{1,0:T(8,128)S(1)} collective-permute-done((f32[32,512]{1,0:T(8,128)S(1)}, f32[32,512]{1,0:T(8,128)S(1)}, u32[]{:S(2)}, u32[]{:S(2)}) %collective-permute-start.6) | collective-permute-done | bytes 65568 | tf_op jit(solution)/shard_map/ppermute | solution.py:519
  279.5 3.0 %collective-permute-done.8 = f32[8,128]{1,0:T(8,128)S(1)} collective-permute-done((f32[8,128]{1,0:T(8,128)S(1)}, f32[8,128]{1,0:T(8,128)S(1)}, u32[]{:S(2)}, u32[]{:S(2)}) %collective-permute-start.8) | collective-permute-done | bytes 4128 | tf_op jit(solution)/shard_map/ppermute | solution.py:519
  288.7 3.1 %assemble.1 = bf16[2048,512]{1,0:T(8,128)(2,1)} custom-call(s32[16]{0:T(128)} %broadcast_xor_fusion.1.owner_ref, bf16[4,128,512]{2,1,0:T(8,128)(2,1)} %copy-done.2, bf16[4,128,512]{2,1,0:T(8,128)(2,1)} %collective-permute-done.29.refs_1_, bf16[4,128,512]{2,1,0:T(8,128)(2,1)} %copy-done.3, bf16[4,128,512]{2,1,0:T(8,128)(2,1)} %collective-permute-done.31.refs_3_), custom_call_target="tpu_custom_call" | custom-call | bytes 4194304 | tf_op jit(solution)/shard_map/assemble/pallas_call | solution.py:504
  293.3 5.4 %out_final.1 = (bf16[512,2048]{1,0:T(8,128)(2,1)}, f32[512,256]{1,0:T(8,128)}, f32[512,256]{1,0:T(8,128)}) custom-call(s32[16]{0:T(128)} %broadcast_xor_fusion.1.owner_ref, f32[8,128]{1,0:T(8,128)} %add.75.sum_ref, s32[8]{0:T(128)} %broadcast_xor_fusion.rank_owner_ref.owner_ref, bf16[2048,256]{1,0:T(8,128)(2,1)} %basis_ref.7, f32[4,256,256]{2,1,0:T(8,128)} %copy-done, ...), custom_call_target="tpu_custom_call" | custom-call | flops 1073741824 | bytes 6291456 | tf_op jit(solution)/shard_map/out_final/pallas_call | solution.py:342
  (136 shorter events, 48.3 us)
Async XLA Ops:
  11.1 79.5 %collective-permute-start.16 = (f32[128,512]{1,0:T(8,128)S(1)}, f32[128,512]{1,0:T(8,128)S(1)}, u32[]{:S(2)}, u32[]{:S(2)}) collective-permute-start(f32[128,512]{1,0:T(8,128)S(1)} %bitcast.30), channel_id=1, source_target_pairs={{0,4},{4,0},{8,12},{12,8},{16,20},{20,16},{24,28},{28,24},{1,5},{5... | collective-permute-start | bytes 786440 | tf_op jit(solution)/shard_map/ppermute | solution.py:519
  93.1 68.0 %collective-permute-start.19 = (f32[32,512]{1,0:T(8,128)}, f32[32,512]{1,0:T(8,128)S(1)}, u32[]{:S(2)}, u32[]{:S(2)}) collective-permute-start(f32[32,512]{1,0:T(8,128)} %get-tuple-element.40), channel_id=1, source_target_pairs={{0,24},{4,28},{8,16},{12,20},{16,8},{20,12},{24,0},{28,4},{1,25},{... | collective-permute-start | bytes 196616 | tf_op jit(solution)/shard_map/ppermute | solution.py:519
  96.7 64.5 %collective-permute-start.18 = (f32[32,512]{1,0:T(8,128)}, f32[32,512]{1,0:T(8,128)S(1)}, u32[]{:S(2)}, u32[]{:S(2)}) collective-permute-start(f32[32,512]{1,0:T(8,128)} %get-tuple-element.39), channel_id=1, source_target_pairs={{0,16},{4,20},{8,24},{12,28},{16,0},{20,4},{24,8},{28,12},{1,17},{... | collective-permute-start | bytes 196616 | tf_op jit(solution)/shard_map/ppermute | solution.py:519
  96.7 64.4 %collective-permute-start.17 = (f32[32,512]{1,0:T(8,128)}, f32[32,512]{1,0:T(8,128)S(1)}, u32[]{:S(2)}, u32[]{:S(2)}) collective-permute-start(f32[32,512]{1,0:T(8,128)} %get-tuple-element.38), channel_id=1, source_target_pairs={{0,8},{4,12},{8,0},{12,4},{16,24},{20,28},{24,16},{28,20},{1,9},{5... | collective-permute-start | bytes 196616 | tf_op jit(solution)/shard_map/ppermute | solution.py:519
  161.9 7.5 %collective-permute-start.20 = (f32[32,512]{1,0:T(8,128)S(1)}, f32[32,512]{1,0:T(8,128)S(1)}, u32[]{:S(2)}, u32[]{:S(2)}) collective-permute-start(f32[32,512]{1,0:T(8,128)S(1)} %get-tuple-element.46.refs_0_), channel_id=1, source_target_pairs={{0,8},{4,12},{8,0},{12,4},{16,24},{20,28},{24,16},{28,20},{1,9},{5... | collective-permute-start | bytes 196616 | tf_op jit(solution)/shard_map/ppermute | solution.py:519
  163.2 18.7 %collective-permute-start.21 = (f32[32,512]{1,0:T(8,128)S(1)}, f32[32,512]{1,0:T(8,128)S(1)}, u32[]{:S(2)}, u32[]{:S(2)}) collective-permute-start(f32[32,512]{1,0:T(8,128)S(1)} %get-tuple-element.46.refs_0_), channel_id=1, source_target_pairs={{0,16},{4,20},{8,24},{12,28},{16,0},{20,4},{24,8},{28,12},{1,17},{... | collective-permute-start | bytes 196616 | tf_op jit(solution)/shard_map/ppermute | solution.py:519
  166.1 15.8 %collective-permute-start.22 = (f32[32,512]{1,0:T(8,128)S(1)}, f32[32,512]{1,0:T(8,128)S(1)}, u32[]{:S(2)}, u32[]{:S(2)}) collective-permute-start(f32[32,512]{1,0:T(8,128)S(1)} %get-tuple-element.46.refs_0_), channel_id=1, source_target_pairs={{0,24},{4,28},{8,16},{12,20},{16,8},{20,12},{24,0},{28,4},{1,25},{... | collective-permute-start | bytes 196616 | tf_op jit(solution)/shard_map/ppermute | solution.py:519
  167.3 21.5 %collective-permute-start = (f32[128,512]{1,0:T(8,128)S(1)}, f32[128,512]{1,0:T(8,128)S(1)}, u32[]{:S(2)}, u32[]{:S(2)}) collective-permute-start(f32[128,512]{1,0:T(8,128)S(1)} %bitcast.31), channel_id=1, source_target_pairs={{0,4},{4,0},{8,12},{12,8},{16,20},{20,16},{24,28},{28,24},{1,5},{5... | collective-permute-start | bytes 786440 | tf_op jit(solution)/shard_map/ppermute | solution.py:519
  167.7 30.7 %collective-permute-start.10 = (f32[512,256]{1,0:T(8,128)S(1)}, f32[512,256]{1,0:T(8,128)S(1)}, u32[]{:S(2)}, u32[]{:S(2)}) collective-permute-start(f32[512,256]{1,0:T(8,128)S(1)} %copy-done.8), channel_id=1, source_target_pairs={{0,16},{4,20},{8,24},{12,28},{16,0},{20,4},{24,8},{28,12},{1,17},{... | collective-permute-start | bytes 1572872 | tf_op jit(solution)/shard_map/ppermute | solution.py:519
  186.7 7.4 %collective-permute-start.24 = (f32[8,128]{1,0:T(8,128)S(1)}, f32[8,128]{1,0:T(8,128)S(1)}, u32[]{:S(2)}, u32[]{:S(2)}) collective-permute-start(f32[8,128]{1,0:T(8,128)S(1)} %add.82), channel_id=1, source_target_pairs={{0,2},{1,3},{2,0},{3,1},{4,6},{5,7},{6,4},{7,5},{8,10},{9,11},{10,... | collective-permute-start | bytes 12296 | tf_op jit(solution)/shard_map/ppermute | solution.py:519
  191.3 38.3 %collective-permute-start.3 = (f32[32,512]{1,0:T(8,128)}, f32[32,512]{1,0:T(8,128)S(1)}, u32[]{:S(2)}, u32[]{:S(2)}) collective-permute-start(f32[32,512]{1,0:T(8,128)} %get-tuple-element.35), channel_id=1, source_target_pairs={{0,24},{4,28},{8,16},{12,20},{16,8},{20,12},{24,0},{28,4},{1,25},{... | collective-permute-start | bytes 196616 | tf_op jit(solution)/shard_map/ppermute | solution.py:519
  193.7 37.7 %collective-permute-start.2 = (f32[32,512]{1,0:T(8,128)}, f32[32,512]{1,0:T(8,128)S(1)}, u32[]{:S(2)}, u32[]{:S(2)}) collective-permute-start(f32[32,512]{1,0:T(8,128)} %get-tuple-element.34), channel_id=1, source_target_pairs={{0,16},{4,20},{8,24},{12,28},{16,0},{20,4},{24,8},{28,12},{1,17},{... | collective-permute-start | bytes 196616 | tf_op jit(solution)/shard_map/ppermute | solution.py:519
  195.1 9.2 %collective-permute-start.26 = (f32[128,512]{1,0:T(8,128)S(1)}, f32[128,512]{1,0:T(8,128)S(1)}, u32[]{:S(2)}, u32[]{:S(2)}) collective-permute-start(f32[128,512]{1,0:T(8,128)S(1)} %pad_maximum_fusion.7.refs_0_), channel_id=1, source_target_pairs={{0,4},{4,0},{8,12},{12,8},{16,20},{20,16},{24,28},{28,24},{1,5},{5... | collective-permute-start | bytes 786440 | tf_op jit(solution)/shard_map/ppermute | solution.py:519
  198.5 21.3 %collective-permute-start.11 = (f32[2,256,256]{2,1,0:T(8,128)S(1)}, f32[2,256,256]{2,1,0:T(8,128)S(1)}, u32[]{:S(2)}, u32[]{:S(2)}) collective-permute-start(f32[2,256,256]{2,1,0:T(8,128)S(1)} %pad_maximum_fusion.2), channel_id=1, source_target_pairs={{0,4},{4,0},{8,12},{12,8},{16,20},{20,16},{24,28},{28,24},{1,5},{5... | collective-permute-start | bytes 1572872 | tf_op jit(solution)/shard_map/ppermute | solution.py:519
  207.8 11.9 %collective-permute-start.27 = (bf16[256,512]{1,0:T(8,128)(2,1)}, bf16[256,512]{1,0:T(8,128)(2,1)S(1)}, u32[]{:S(2)}, u32[]{:S(2)}) collective-permute-start(bf16[256,512]{1,0:T(8,128)(2,1)} %get-tuple-element.45), channel_id=1, source_target_pairs={{0,16},{4,20},{8,24},{12,28},{16,0},{20,4},{24,8},{28,12},{1,17},{... | collective-permute-start | bytes 786440 | tf_op jit(solution)/shard_map/ppermute | solution.py:519
  210.2 16.8 %collective-permute-start.13 = (f32[2,256,256]{2,1,0:T(8,128)S(1)}, f32[2,256,256]{2,1,0:T(8,128)S(1)}, u32[]{:S(2)}, u32[]{:S(2)}) collective-permute-start(f32[2,256,256]{2,1,0:T(8,128)S(1)} %pad_maximum_fusion.3), channel_id=1, source_target_pairs={{0,8},{4,12},{8,0},{12,4},{16,24},{20,28},{24,16},{28,20},{1,9},{5... | collective-permute-start | bytes 1572872 | tf_op jit(solution)/shard_map/ppermute | solution.py:519
  219.7 11.8 %collective-permute-start.1 = (f32[32,512]{1,0:T(8,128)S(1)}, f32[32,512]{1,0:T(8,128)S(1)}, u32[]{:S(2)}, u32[]{:S(2)}) collective-permute-start(f32[32,512]{1,0:T(8,128)S(1)} %copy-done.25), channel_id=1, source_target_pairs={{0,8},{4,12},{8,0},{12,4},{16,24},{20,28},{24,16},{28,20},{1,9},{5... | collective-permute-start | bytes 196616 | tf_op jit(solution)/shard_map/ppermute | solution.py:519
  219.8 14.4 %collective-permute-start.28 = (bf16[2,128,512]{2,1,0:T(8,128)(2,1)S(1)}, bf16[2,128,512]{2,1,0:T(8,128)(2,1)S(1)}, u32[]{:S(2)}, u32[]{:S(2)}) collective-permute-start(bf16[2,128,512]{2,1,0:T(8,128)(2,1)S(1)} %pad_maximum_fusion.8), channel_id=1, source_target_pairs={{0,4},{4,0},{8,12},{12,8},{16,20},{20,16},{24,28},{28,24},{1,5},{5... | collective-permute-start | bytes 786440 | tf_op jit(solution)/shard_map/ppermute | solution.py:519
  227.1 65.5 %collective-permute-start.12 = (f32[4,256,256]{2,1,0:T(8,128)S(1)}, f32[4,256,256]{2,1,0:T(8,128)}, u32[]{:S(2)}, u32[]{:S(2)}) collective-permute-start(f32[4,256,256]{2,1,0:T(8,128)S(1)} %pad_maximum_fusion.refs_0_), channel_id=1, source_target_pairs={{0,8},{4,12},{8,0},{12,4},{16,24},{20,28},{24,16},{28,20},{1,9},{5... | collective-permute-start | bytes 3145736 | tf_op jit(solution)/shard_map/ppermute | solution.py:519
  229.7 62.9 %collective-permute-start.14 = (f32[4,256,256]{2,1,0:T(8,128)S(1)}, f32[4,256,256]{2,1,0:T(8,128)}, u32[]{:S(2)}, u32[]{:S(2)}) collective-permute-start(f32[4,256,256]{2,1,0:T(8,128)S(1)} %pad_maximum_fusion.1.refs_2_), channel_id=1, source_target_pairs={{0,4},{4,0},{8,12},{12,8},{16,20},{20,16},{24,28},{28,24},{1,5},{5... | collective-permute-start | bytes 3145736 | tf_op jit(solution)/shard_map/ppermute | solution.py:519
  231.4 28.5 %collective-permute-start.30 = (bf16[2,128,512]{2,1,0:T(8,128)(2,1)S(1)}, bf16[2,128,512]{2,1,0:T(8,128)(2,1)S(1)}, u32[]{:S(2)}, u32[]{:S(2)}) collective-permute-start(bf16[2,128,512]{2,1,0:T(8,128)(2,1)S(1)} %pad_maximum_fusion.9), channel_id=1, source_target_pairs={{0,8},{4,12},{8,0},{12,4},{16,24},{20,28},{24,16},{28,20},{1,9},{5... | collective-permute-start | bytes 786440 | tf_op jit(solution)/shard_map/ppermute | solution.py:519
  232.2 29.4 %collective-permute-start.4 = (f32[32,512]{1,0:T(8,128)S(1)}, f32[32,512]{1,0:T(8,128)S(1)}, u32[]{:S(2)}, u32[]{:S(2)}) collective-permute-start(f32[32,512]{1,0:T(8,128)S(1)} %get-tuple-element.49.refs_0_), channel_id=1, source_target_pairs={{0,8},{4,12},{8,0},{12,4},{16,24},{20,28},{24,16},{28,20},{1,9},{5... | collective-permute-start | bytes 196616 | tf_op jit(solution)/shard_map/ppermute | solution.py:519
  234.3 54.4 %collective-permute-start.29 = (bf16[4,128,512]{2,1,0:T(8,128)(2,1)S(1)}, bf16[4,128,512]{2,1,0:T(8,128)(2,1)}, u32[]{:S(2)}, u32[]{:S(2)}) collective-permute-start(bf16[4,128,512]{2,1,0:T(8,128)(2,1)S(1)} %pad_maximum_fusion.4.refs_0_), channel_id=1, source_target_pairs={{0,8},{4,12},{8,0},{12,4},{16,24},{20,28},{24,16},{28,20},{1,9},{5... | collective-permute-start | bytes 1572872 | tf_op jit(solution)/shard_map/ppermute | solution.py:519
  259.9 28.8 %collective-permute-start.31 = (bf16[4,128,512]{2,1,0:T(8,128)(2,1)S(1)}, bf16[4,128,512]{2,1,0:T(8,128)(2,1)}, u32[]{:S(2)}, u32[]{:S(2)}) collective-permute-start(bf16[4,128,512]{2,1,0:T(8,128)(2,1)S(1)} %pad_maximum_fusion.5.refs_2_), channel_id=1, source_target_pairs={{0,4},{4,0},{8,12},{12,8},{16,20},{20,16},{24,28},{28,24},{1,5},{5... | collective-permute-start | bytes 1572872 | tf_op jit(solution)/shard_map/ppermute | solution.py:519
  (36 other events, 711.7 us)
where the time goes:
time: 300 us; the launch traced here: 299 us
  Pallas kernels  167 us (56%)
  waiting for transfers between devices  75.8 us (25%)
  starting transfers between devices  39.3 us (13%)
  other arithmetic  7.95 us (3%)
  local copies, waits for them, and re-layouts  7.74 us (3%)
    pallas_call x3, Pallas kernels, attend_heads(): pl.pallas_call(functools.partial(attend_kernel, bq, start), grid=(count,)...  131 us
    ppermute x32, waiting for transfers between devices, swap(): return lax.ppermute(x, axis, [(i, i ^ bit) for i in range(n)])  75.8 us
    ppermute x32, starting transfers between devices, swap(): return lax.ppermute(x, axis, [(i, i ^ bit) for i in range(n)])  39.3 us
    pallas_call x1, Pallas kernels, value_proj(): pl.pallas_call(value_proj_kernel, grid=(tokens // block,), out_shape=jax....  9.42 us
    pallas_call x2, Pallas kernels, low_rank_rows(): pl.pallas_call(low_rank_kernel, grid=(tokens // block,), out_shape=(out,...  8.48 us
  transfers between devices with their start and end apart: 32, of which 13 were waited for; matrix products, arithmetic and copies ran while one was open for 3% of the time, Pallas kernels for 50%

commit v1 on v0

--- a/solution.py
+++ b/solution.py
@@ -29,7 +29,17 @@
     return high, (x - high.astype(F32)).astype(BF16)
 
 
-def value_proj_kernel(x_ref, c_ref, basis_ref, proj_ref):
+def write_sends(place_ref, outer, proj_ref, send_refs):
+    inner = len(send_refs) + 1
+    rows = proj_ref.shape[0] // (outer * inner)
+    for d, send_ref in enumerate(send_refs, 1):
+        member = place_ref[0] ^ d
+        for p in range(outer):
+            at = pl.multiple_of((p * inner + member) * rows, rows)
+            send_ref[p * rows : (p + 1) * rows, :] = proj_ref[pl.ds(at, rows), :]
+
+
+def value_proj_kernel(outer, place_ref, x_ref, c_ref, basis_ref, proj_ref, *send_refs):
     y = jnp.dot(x_ref[...], basis_ref[...], preferred_element_type=F32)
     high, low = split_pair(y.T)
     part = jnp.dot(high, c_ref[...], preferred_element_type=F32) + jnp.dot(
@@ -45,20 +55,33 @@
         proj_ref[...] += part
 
 
-def value_proj(x, c, basis):
+    @pl.when(pl.program_id(0) == pl.num_programs(0) - 1)
+    def _():
+        write_sends(place_ref, outer, proj_ref, send_refs)
+
+
+def sends_shape(rank, cols):
+    _, inner = groups_of("fs")
+    return [jax.ShapeDtypeStruct((rank // inner, cols), F32)] * (inner - 1)
+
+
+def value_proj(place, x, c, basis):
     tokens, width = x.shape
     rank, cols = basis.shape[1], c.shape[1]
     block = min(512, tokens)
-    return pl.pallas_call(
-        value_proj_kernel,
+    outer, inner = groups_of("fs")
+    return pl.pallas_call(
+        functools.partial(value_proj_kernel, outer),
         grid=(tokens // block,),
-        out_shape=jax.ShapeDtypeStruct((rank, cols), F32),
+        out_shape=[jax.ShapeDtypeStruct((rank, cols), F32)] + sends_shape(rank, cols),
         in_specs=[
+            pl.BlockSpec(memory_space=pltpu.SMEM),
             pl.BlockSpec((block, width), lambda t: (t, 0)),
             pl.BlockSpec((block, cols), lambda t: (t, 0)),
             pl.BlockSpec((width, rank), lambda t: (0, 0)),
         ],
-        out_specs=pl.BlockSpec((rank, cols), lambda t: (0, 0)),
+        out_specs=[pl.BlockSpec((rank, cols), lambda t: (0, 0))]
+        + [pl.BlockSpec((rank // inner, cols), lambda t: (0, 0))] * (inner - 1),
         cost_estimate=pl.CostEstimate(
             flops=2 * tokens * rank * (width + 2 * cols),
             bytes_accessed=2 * tokens * (width + cols),
@@ -66,14 +89,12 @@
         ),
         compiler_params=pltpu.CompilerParams(vmem_limit_bytes=VMEM_BYTES),
         name="value_proj",
-    )(x, c, basis)
+    )(place, x, c, basis)
 
 
 def low_rank_kernel(x_ref, basis_ref, high_ref, low_ref):
     y = jnp.dot(x_ref[...], basis_ref[...], preferred_element_type=F32)
-    high, low = split_pair(y.T)
-    high_ref[...] = high
-    low_ref[...] = low
+    high_ref[...], low_ref[...] = split_pair(y)
 
 
 def low_rank_rows(half, x, basis):
@@ -81,7 +102,7 @@
     rank = basis.shape[1]
     block = min(512, tokens)
     skip = half * (tokens // block)
-    out = jax.ShapeDtypeStruct((rank, tokens), BF16)
+    out = jax.ShapeDtypeStruct((tokens, rank), BF16)
     return pl.pallas_call(
         low_rank_kernel,
         grid=(tokens // block,),
@@ -90,7 +111,7 @@
             pl.BlockSpec((block, width), lambda t: (t + skip, 0)),
             pl.BlockSpec((width, rank), lambda t: (0, 0)),
         ],
-        out_specs=[pl.BlockSpec((rank, block), lambda t: (0, t))] * 2,
+        out_specs=[pl.BlockSpec((block, rank), lambda t: (t, 0))] * 2,
         cost_estimate=pl.CostEstimate(
             flops=2 * tokens * rank * width,
             bytes_accessed=2 * tokens * width,
@@ -102,12 +123,11 @@
 
 
 def attend_kernel(
-    bq, start, lam_ref, gain_ref, q_hbm, k_hbm, v_hbm, high_hbm, low_hbm, high_two,
-    low_two, *rest
+    bq, start, outer, inner, place_ref, lam_ref, gain_ref, q_hbm, k_hbm, v_hbm, high_hbm,
+    low_hbm, high_two, low_two, *rest
 ):
-    proj_ref, q_all, k_all, v_all, high_ref, low_ref, e_ref, h_ref, sum_ref, sems, late_sems = (
-        rest[-11:]
-    )
+    q_all, k_all, v_all, high_ref, low_ref, e_ref, h_ref, sum_ref, sems, late_sems = rest[-10:]
+    proj_ref, *send_refs = rest[-10 - inner : -10]
     count, seq, width = q_all.shape
     step = pl.program_id(0)
 
@@ -125,7 +145,7 @@
         return [
             pltpu.make_async_copy(
                 source,
-                target.at[:, pl.ds(i // 2 * (seq // 2), seq // 2)],
+                target.at[pl.ds(i // 2 * (seq // 2), seq // 2), :],
                 late_sems.at[i],
             )
             for i, (source, target) in enumerate(pairs)
@@ -135,78 +155,69 @@
     def _():
         for copy in head_copies(0):
             copy.start()
+
+    for copy in head_copies(step):
+        copy.wait()
+
+    @pl.when(step == 0)
+    def _():
         for copy in late_copies():
             copy.start()
         for j in range(1, count):
             for copy in head_copies(j):
                 copy.start()
 
-    for copy in head_copies(step):
-        copy.wait()
     q_ref, k_ref, v_ref = q_all.at[step], k_all.at[step], v_all.at[step]
     half = width // 2
     lam = lam_ref[start + step]
     scale = half**-0.5
     first = lax.broadcasted_iota(jnp.int32, (1, width), 1) < half
 
-    mark = (
-        lax.broadcasted_iota(jnp.int32, (width, 128), 0) // half
-        == lax.broadcasted_iota(jnp.int32, (width, 128), 1) // 64
-    ).astype(BF16)
-
-    def top_norm(ref):
-        x = ref[...]
-        return jnp.max(
-            jnp.dot(x * x, mark, preferred_element_type=F32), axis=0, keepdims=True
-        )
-
-    bound = jnp.max(top_norm(q_ref) * top_norm(k_ref))
-    small = bound < (70.0 / scale) ** 2
-
     def finish(base, rows, mix, values):
         raw = jnp.dot(mix, values, preferred_element_type=F32)
         square = jnp.mean(raw * raw, axis=-1, keepdims=True)
         normed = raw * lax.rsqrt(square + EPSILON_NORM) * gain_ref[...]
-        h_ref[pl.ds(base, rows), :] = normed.astype(BF16)
-
-    @pl.when(small)
+        h_ref[:, pl.ds(base, rows)] = normed.T.astype(BF16)
+
+    keep = lax.broadcasted_iota(jnp.int32, (bq, bq), 1) <= lax.broadcasted_iota(
+        jnp.int32, (bq, bq), 0
+    )
+    keep_both = jnp.concatenate([keep, keep], axis=0)
+    for i in range(seq // bq):
+        slot = i % 2
+        q = q_ref[i * bq : (i + 1) * bq, :]
+        zero = jnp.zeros_like(q)
+        both = jnp.concatenate(
+            [jnp.where(first, q, zero), jnp.where(first, zero, q)], axis=0
+        )
+        for t in range(i + 1):
+            scores = lax.dot_general(
+                both, k_ref[t * bq : (t + 1) * bq, :], NT, preferred_element_type=F32
+            )
+            e = jnp.exp2(scores * (scale * LOG2E))
+            if t == i:
+                e = jnp.where(keep_both, e, 0.0)
+            e_ref[slot, :, t * bq : (t + 1) * bq] = e
+            part = e[:, :128]
+            for c in range(1, bq // 128):
+                part = part + e[:, c * 128 : (c + 1) * 128]
+            if t == 0:
+                sum_ref[slot] = part
+            else:
+                sum_ref[slot] += part
+        total = jnp.sum(sum_ref[slot], axis=-1, keepdims=True)
+        most = total if i == 0 else jnp.maximum(most, total)
+        least = total if i == 0 else jnp.minimum(least, total)
+        one = 1.0 / total[:bq]
+        two = lam / total[bq:]
+        n = (i + 1) * bq
+        mix = e_ref[slot, :bq, :n] * one - e_ref[slot, bq:, :n] * two
+        finish(i * bq, bq, mix.astype(BF16), v_ref[:n, :])
+    fine = (jnp.max(most) < 2.0**120) & (jnp.min(least) > 2.0**-60)
+
+    @pl.when(jnp.logical_not(fine))
     def _():
-        keep = lax.broadcasted_iota(jnp.int32, (bq, bq), 1) <= lax.broadcasted_iota(
-            jnp.int32, (bq, bq), 0
-        )
-        keep_both = jnp.concatenate([keep, keep], axis=0)
-        for i in range(seq // bq):
-            slot = i % 2
-            q = q_ref[i * bq : (i + 1) * bq, :]
-            zero = jnp.zeros_like(q)
-            both = jnp.concatenate(
-                [jnp.where(first, q, zero), jnp.where(first, zero, q)], axis=0
-            )
-            for t in range(i + 1):
-                scores = lax.dot_general(
-                    both, k_ref[t * bq : (t + 1) * bq, :], NT, preferred_element_type=F32
-                )
-                e = jnp.exp2(scores * (scale * LOG2E))
-                if t == i:
-                    e = jnp.where(keep_both, e, 0.0)
-                e_ref[slot, :, t * bq : (t + 1) * bq] = e
-                part = e[:, :128]
-                for c in range(1, bq // 128):
-                    part = part + e[:, c * 128 : (c + 1) * 128]
-                if t == 0:
-                    sum_ref[slot] = part
-                else:
-                    sum_ref[slot] += part
-            total = jnp.sum(sum_ref[slot], axis=-1, keepdims=True)
-            one = 1.0 / total[:bq]
-            two = lam / total[bq:]
-            n = (i + 1) * bq
-            mix = e_ref[slot, :bq, :n] * one - e_ref[slot, bq:, :n] * two
-            finish(i * bq, bq, mix.astype(BF16), v_ref[:n, :])
-
-    @pl.when(jnp.logical_not(small))
-    def _():
-        few = min(64, bq)
+        few = min(128, bq)
 
         def block(i, carry):
             base = pl.multiple_of(i * few, few)
@@ -239,39 +250,47 @@
             copy.wait()
 
     h = h_ref[...]
-    proj_ref[...] = jnp.dot(high_ref[...], h, preferred_element_type=F32) + jnp.dot(
-        low_ref[...], h, preferred_element_type=F32
-    )
-
-
-def attend_heads(start, stop, query_rows, key_rows, value_rows, mix_lambda, head_gain, pairs, prev):
+    turned = jnp.dot(h, high_ref[...], preferred_element_type=F32) + jnp.dot(
+        h, low_ref[...], preferred_element_type=F32
+    )
+    proj_ref[...] = turned.T
+    write_sends(place_ref, outer, proj_ref, send_refs)
+
+
+def attend_heads(
+    start, stop, place, query_rows, key_rows, value_rows, mix_lambda, head_gain, pairs,
+    earlier,
+):
     seq = query_rows.shape[0]
     heads = mix_lambda.shape[0]
     count = stop - start
     width = query_rows.shape[1] // heads
-    rank = pairs[0][0].shape[0]
+    rank = pairs[0][0].shape[1]
     bq = min(256, seq)
+    outer, inner = groups_of("fs")
     hbm = pl.BlockSpec(memory_space=pl.ANY)
-    earlier = () if prev is None else (prev,)
-    return pl.pallas_call(
-        functools.partial(attend_kernel, bq, start),
+    return pl.pallas_call(
+        functools.partial(attend_kernel, bq, start, outer, inner),
         grid=(count,),
-        out_shape=jax.ShapeDtypeStruct((rank, heads * DV), F32),
+        out_shape=[jax.ShapeDtypeStruct((rank, heads * DV), F32)]
+        + sends_shape(rank, heads * DV),
         in_specs=[
+            pl.BlockSpec(memory_space=pltpu.SMEM),
             pl.BlockSpec(memory_space=pltpu.SMEM),
             pl.BlockSpec(memory_space=pltpu.VMEM),
         ]
         + [hbm] * (7 + len(earlier)),
-        out_specs=pl.BlockSpec((rank, DV), lambda j: (0, j + start)),
-        input_output_aliases={9: 0} if earlier else {},
+        out_specs=[pl.BlockSpec((rank, DV), lambda j: (0, j + start))]
+        + [pl.BlockSpec((rank // inner, DV), lambda j: (0, j + start))] * (inner - 1),
+        input_output_aliases={10 + i: i for i in range(len(earlier))},
         scratch_shapes=[
             pltpu.VMEM((count, seq, width), BF16),
             pltpu.VMEM((count, seq, width), BF16),
             pltpu.VMEM((count, seq, DV), BF16),
-            pltpu.VMEM((rank, seq), BF16),
-            pltpu.VMEM((rank, seq), BF16),
+            pltpu.VMEM((seq, rank), BF16),
+            pltpu.VMEM((seq, rank), BF16),
             pltpu.VMEM((2, 2 * bq, seq), F32),
-            pltpu.VMEM((seq, DV), BF16),
+            pltpu.VMEM((DV, seq), BF16),
             pltpu.VMEM((2, 2 * bq, 128), F32),
             pltpu.SemaphoreType.DMA((count, 3)),
             pltpu.SemaphoreType.DMA((4,)),
@@ -284,6 +303,7 @@
         compiler_params=pltpu.CompilerParams(vmem_limit_bytes=VMEM_BYTES),
         name="attend_heads",
     )(
+        place,
         mix_lambda,
         head_gain.reshape(1, DV),
         query_rows,
@@ -530,17 +550,12 @@
     return outer, n // outer
 
 
-def reduce_scatter(x, axis):
+def reduce_scatter(x, sends, axis):
     outer, inner = groups_of(axis)
     me = lax.axis_index(axis)
-    rows, cols = x.shape[0] // (outer * inner), x.shape[1]
-    place_out, place_in = me // inner, me % inner
-    blocks = x.reshape(outer, inner, rows, cols)
-    arrived = []
-    for d in range(1, inner):
-        send = lax.dynamic_index_in_dim(blocks, place_in ^ d, 1, keepdims=False)
-        arrived.append(swap(send.reshape(outer * rows, cols), axis, d))
-    sums = fold(x, arrived, place_in, inner, place_out, outer, rows)
+    rows = x.shape[0] // (outer * inner)
+    arrived = [swap(send, axis, d) for d, send in enumerate(sends, 1)]
+    sums = fold(x, arrived, me % inner, inner, me // inner, outer, rows)
     total = sums[0]
     for d in range(1, outer):
         total = total + swap(sums[d], axis, d * inner)
@@ -613,8 +628,9 @@
     me = lax.axis_index("fs")
     parts, owners = gather_by_distance(out_weight, "fs")
 
-    value_part = value_proj(layer_input, value_cotangent, value_basis)
-    value_sum = reduce_scatter(value_part, "fs")
+    place = (me % groups_of("fs")[1]).reshape(1)
+    value_part, *value_sends = value_proj(place, layer_input, value_cotangent, value_basis)
+    value_sum = reduce_scatter(value_part, value_sends, "fs")
     new_value_first, new_value_second, value_dir = moment_step(
         value_sum, value_first, value_second
     )
@@ -626,14 +642,14 @@
 
     pairs = [low_rank_rows(half, out_cotangent, out_basis) for half in range(2)]
     heads = mix_lambda.shape[0]
-    out_part = None
+    out_parts = ()
     cuts = sorted({0, heads // 4, heads // 2, heads})
     for start, stop in zip(cuts[:-1], cuts[1:]):
-        out_part = attend_heads(
-            start, stop, query_rows, key_rows,
-            value_rows, mix_lambda, head_gain, pairs, out_part,
+        out_parts = attend_heads(
+            start, stop, place, query_rows, key_rows, value_rows, mix_lambda,
+            head_gain, pairs, out_parts,
         )
-    out_sum = reduce_scatter(out_part, "fs")
+    out_sum = reduce_scatter(out_parts[0], out_parts[1:], "fs")
     new_out_first, new_out_second, out_dir = moment_step(out_sum, out_first, out_second)
     out_dirs, out_owners, *out_squares = gather_and_square(out_dir)
     out_copy, out_step, new_out_weight = out_final(

time: 300 us -> 281 us (0.937)
  Pallas kernels: 167 us -> 158 us
  waiting for transfers between devices: 75.8 us -> 69.2 us
    pallas_call x4, Pallas kernels: 140 us -> 132 us  [the longest x3 123 us: attend_heads(): pl.pallas_call(functools.partial(attend_kernel, bq, start, outer, inner),...]
    ppermute x32, waiting for transfers between devices: 75.8 us -> 69.2 us  [swap(): return lax.ppermute(x, axis, [(i, i ^ bit) for i in range(n)])]
  transfers between devices with their start and end apart: 32 -> 32, of which waited for: 13 -> 13; matrix products, arithmetic and copies ran while one was open for 3% -> 3% of each run, Pallas kernels for 50% -> 51%
where the time goes in v1:
time: 281 us; the launch traced here: 280 us
  Pallas kernels  158 us (56%)
  waiting for transfers between devices  69.2 us (25%)
  starting transfers between devices  37.4 us (13%)
  other arithmetic  7.9 us (3%)
  local copies, waits for them, and re-layouts  5.85 us (2%)
    pallas_call x3, Pallas kernels, attend_heads(): pl.pallas_call(functools.partial(attend_kernel, bq, start, outer, inner),...  123 us
    ppermute x32, waiting for transfers between devices, swap(): return lax.ppermute(x, axis, [(i, i ^ bit) for i in range(n)])  69.2 us
    ppermute x32, starting transfers between devices, swap(): return lax.ppermute(x, axis, [(i, i ^ bit) for i in range(n)])  37.4 us
    pallas_call x1, Pallas kernels, value_proj(): pl.pallas_call(functools.partial(value_proj_kernel, outer), grid=(tokens...  9.55 us
    pallas_call x2, Pallas kernels, low_rank_rows(): pl.pallas_call(low_rank_kernel, grid=(tokens // block,), out_shape=(out,...  8.2 us
  transfers between devices with their start and end apart: 32, of which 13 were waited for; matrix products, arithmetic and copies ran while one was open for 3% of the time, Pallas kernels for 51%

profile of v1, /device:TPU:0, one launch (start us, length us, event | category | flops | bytes accessed | tf_op | source)
XLA Modules:
  0.0 280.1 jit_solution(447780118069658449)
XLA Ops:
  0.7 9.6 %value_proj.1 = (f32[256,512]{1,0:T(8,128)}, f32[128,512]{1,0:T(8,128)}) custom-call(s32[1]{0:T(128)} %bitcast.place_ref, bf16[2048,2048]{1,0:T(8,128)(2,1)} %x_ref.5, bf16[2048,512]{1,0:T(8,128)(2,1)} %c_ref.1, bf16[2048,256]{1,0:T(8,128)(2,1)} %basis_ref.9), custom_call_target="tpu_custom_call" | custom-call | flops 3221225472 | bytes 10485760 | tf_op jit(solution)/shard_map/value_proj/pallas_call | solution.py:73
  10.2 3.0 %collective-permute-start.16 = (f32[128,512]{1,0:T(8,128)}, f32[128,512]{1,0:T(8,128)S(1)}, u32[]{:S(2)}, u32[]{:S(2)}) collective-permute-start(f32[128,512]{1,0:T(8,128)} %get-tuple-element.52), channel_id=1, source_target_pairs={{0,4},{4,0},{8,12},{12,8},{16,20},{20,16},{24,28},{28,24},{1,5},{5... | collective-permute-start | bytes 786440 | tf_op jit(solution)/shard_map/ppermute | solution.py:539
  13.2 4.1 %low_rank_rows.2 = (bf16[1024,256]{1,0:T(8,128)(2,1)}, bf16[1024,256]{1,0:T(8,128)(2,1)}) custom-call(bf16[2048,2048]{1,0:T(8,128)(2,1)} %x_ref.4, bf16[2048,256]{1,0:T(8,128)(2,1)} %basis_ref.7), custom_call_target="tpu_custom_call" | custom-call | flops 1073741824 | bytes 4194304 | tf_op jit(solution)/shard_map/low_rank_rows/pallas_call | solution.py:106
  17.3 4.1 %low_rank_rows.3 = (bf16[1024,256]{1,0:T(8,128)(2,1)}, bf16[1024,256]{1,0:T(8,128)(2,1)}) custom-call(bf16[2048,2048]{1,0:T(8,128)(2,1)} %x_ref.4, bf16[2048,256]{1,0:T(8,128)(2,1)} %basis_ref.7), custom_call_target="tpu_custom_call" | custom-call | flops 1073741824 | bytes 4194304 | tf_op jit(solution)/shard_map/low_rank_rows/pallas_call | solution.py:106
  21.9 31.5 %attend_heads.3 = (f32[256,512]{1,0:T(8,128)}, f32[128,512]{1,0:T(8,128)}) custom-call(s32[1]{0:T(128)} %bitcast.place_ref, f32[4]{0:T(128)} %lam_ref.5, f32[1,128]{1,0:T(1,128)} %bitcast.20, bf16[2048,512]{1,0:T(8,128)(2,1)} %q_hbm.5, bf16[2048,512]{1,0:T(8,128)(2,1)} %k_hbm.5, bf16[2048,512]{1,0:T(8,128)(2,1)} %v_hbm.5, ...), custom_call_target="tpu_custom_call" | custom-call | flops 4294967296 | bytes 3670016 | tf_op jit(solution)/shard_map/attend_heads/pallas_call | solution.py:272
  56.0 3.6 %collective-permute-start.19 = (f32[32,512]{1,0:T(8,128)}, f32[32,512]{1,0:T(8,128)S(1)}, u32[]{:S(2)}, u32[]{:S(2)}) collective-permute-start(f32[32,512]{1,0:T(8,128)} %get-tuple-element.56), channel_id=1, source_target_pairs={{0,24},{4,28},{8,16},{12,20},{16,8},{20,12},{24,0},{28,4},{1,25},{... | collective-permute-start | bytes 196616 | tf_op jit(solution)/shard_map/ppermute | solution.py:539
  60.4 31.7 %attend_heads.4 = (f32[256,512]{1,0:T(8,128)}, f32[128,512]{1,0:T(8,128)}) custom-call(s32[1]{0:T(128)} %bitcast.place_ref, f32[4]{0:T(128)} %lam_ref.5, f32[1,128]{1,0:T(1,128)} %bitcast.21, bf16[2048,512]{1,0:T(8,128)(2,1)} %q_hbm.5, bf16[2048,512]{1,0:T(8,128)(2,1)} %k_hbm.5, ...), custom_call_target="tpu_custom_call", output_to_operand_aliasing={{0}: (10, {}), {1}: (11, {})} | custom-call | flops 4294967296 | bytes 3670016 | tf_op jit(solution)/shard_map/attend_heads/pallas_call | solution.py:272
  94.1 2.9 %collective-permute-start.21 = (f32[32,512]{1,0:T(8,128)}, f32[32,512]{1,0:T(8,128)S(1)}, u32[]{:S(2)}, u32[]{:S(2)}) collective-permute-start(f32[32,512]{1,0:T(8,128)} %get-tuple-element.62.refs_0_), channel_id=1, source_target_pairs={{0,16},{4,20},{8,24},{12,28},{16,0},{20,4},{24,8},{28,12},{1,17},{... | collective-permute-start | bytes 196616 | tf_op jit(solution)/shard_map/ppermute | solution.py:539
  97.3 59.6 %attend_heads.5 = (f32[256,512]{1,0:T(8,128)}, f32[128,512]{1,0:T(8,128)}) custom-call(s32[1]{0:T(128)} %bitcast.place_ref, f32[4]{0:T(128)} %lam_ref.5, f32[1,128]{1,0:T(1,128)} %bitcast.22, bf16[2048,512]{1,0:T(8,128)(2,1)} %q_hbm.5, bf16[2048,512]{1,0:T(8,128)(2,1)} %k_hbm.5, ...), custom_call_target="tpu_custom_call", output_to_operand_aliasing={{0}: (10, {}), {1}: (11, {})} | custom-call | flops 8589934592 | bytes 5242880 | tf_op jit(solution)/shard_map/attend_heads/pallas_call | solution.py:272
  168.2 2.4 collective-permute-start.3
  176.8 8.1 %collective-permute-done.10 = f32[512,256]{1,0:T(8,128)S(1)} collective-permute-done((f32[512,256]{1,0:T(8,128)S(1)}, f32[512,256]{1,0:T(8,128)S(1)}, u32[]{:S(2)}, u32[]{:S(2)}) %collective-permute-start.10) | collective-permute-done | bytes 524320 | tf_op jit(solution)/shard_map/ppermute | solution.py:539
  187.3 2.7 value_final.1
  190.0 2.1 collective-permute-start.13
  193.1 9.9 %collective-permute-done.27 = bf16[256,512]{1,0:T(8,128)(2,1)S(1)} collective-permute-done((bf16[256,512]{1,0:T(8,128)(2,1)}, bf16[256,512]{1,0:T(8,128)(2,1)S(1)}, u32[]{:S(2)}, u32[]{:S(2)}) %collective-permute-start.27) | collective-permute-done | bytes 262176 | tf_op jit(solution)/shard_map/ppermute | solution.py:539
  203.8 5.5 %collective-permute-done.13 = f32[2,256,256]{2,1,0:T(8,128)S(1)} collective-permute-done((f32[2,256,256]{2,1,0:T(8,128)S(1)}, f32[2,256,256]{2,1,0:T(8,128)S(1)}, u32[]{:S(2)}, u32[]{:S(2)}) %collective-permute-start.13) | collective-permute-done | bytes 524320 | tf_op jit(solution)/shard_map/ppermute | solution.py:539
  210.0 2.1 collective-permute-start.30
  215.0 26.6 %collective-permute-done.30 = bf16[2,128,512]{2,1,0:T(8,128)(2,1)S(1)} collective-permute-done((bf16[2,128,512]{2,1,0:T(8,128)(2,1)S(1)}, bf16[2,128,512]{2,1,0:T(8,128)(2,1)S(1)}, u32[]{:S(2)}, u32[]{:S(2)}) %collective-permute-start.30) | collective-permute-done | bytes 262176 | tf_op jit(solution)/shard_map/ppermute | solution.py:539
  243.3 6.5 %collective-permute-done.5.refs_2_ = f32[32,512]{1,0:T(8,128)S(1)} collective-permute-done((f32[32,512]{1,0:T(8,128)S(1)}, f32[32,512]{1,0:T(8,128)S(1)}, u32[]{:S(2)}, u32[]{:S(2)}) %collective-permute-start.5) | collective-permute-done | bytes 65568 | tf_op jit(solution)/shard_map/ppermute | solution.py:539
  249.9 3.2 %collective-permute-start.6 = (f32[32,512]{1,0:T(8,128)S(1)}, f32[32,512]{1,0:T(8,128)S(1)}, u32[]{:S(2)}, u32[]{:S(2)}) collective-permute-start(f32[32,512]{1,0:T(8,128)S(1)} %get-tuple-element.65.refs_0_), channel_id=1, source_target_pairs={{0,24},{4,28},{8,16},{12,20},{16,8},{20,12},{24,0},{28,4},{1,25},{... | collective-permute-start | bytes 196616 | tf_op jit(solution)/shard_map/ppermute | solution.py:539
  253.1 2.8 %collective-permute-done.6.refs_3_ = f32[32,512]{1,0:T(8,128)S(1)} collective-permute-done((f32[32,512]{1,0:T(8,128)S(1)}, f32[32,512]{1,0:T(8,128)S(1)}, u32[]{:S(2)}, u32[]{:S(2)}) %collective-permute-start.6) | collective-permute-done | bytes 65568 | tf_op jit(solution)/shard_map/ppermute | solution.py:539
  261.7 2.1 collective-permute-done.8
  265.3 2.1 collective-permute-done.9
  269.1 3.1 %assemble.1 = bf16[2048,512]{1,0:T(8,128)(2,1)} custom-call(s32[16]{0:T(128)} %broadcast_xor_fusion.1.owner_ref, bf16[4,128,512]{2,1,0:T(8,128)(2,1)} %copy-done.2, bf16[4,128,512]{2,1,0:T(8,128)(2,1)} %collective-permute-done.29.refs_1_, bf16[4,128,512]{2,1,0:T(8,128)(2,1)} %copy-done.3, bf16[4,128,512]{2,1,0:T(8,128)(2,1)} %collective-permute-done.31.refs_3_), custom_call_target="tpu_custom_call" | custom-call | bytes 4194304 | tf_op jit(solution)/shard_map/assemble/pallas_call | solution.py:524
  274.5 5.4 %out_final.1 = (bf16[512,2048]{1,0:T(8,128)(2,1)}, f32[512,256]{1,0:T(8,128)}, f32[512,256]{1,0:T(8,128)}) custom-call(s32[16]{0:T(128)} %broadcast_xor_fusion.1.owner_ref, f32[8,128]{1,0:T(8,128)} %add.70.sum_ref, s32[8]{0:T(128)} %broadcast_xor_fusion.rank_owner_ref.owner_ref, bf16[2048,256]{1,0:T(8,128)(2,1)} %basis_ref.7, f32[4,256,256]{2,1,0:T(8,128)} %copy-done, ...), custom_call_target="tpu_custom_call" | custom-call | flops 1073741824 | bytes 6291456 | tf_op jit(solution)/shard_map/out_final/pallas_call | solution.py:362
  (132 shorter events, 44.2 us)
Async XLA Ops:
  10.2 43.2 %collective-permute-start.16 = (f32[128,512]{1,0:T(8,128)}, f32[128,512]{1,0:T(8,128)S(1)}, u32[]{:S(2)}, u32[]{:S(2)}) collective-permute-start(f32[128,512]{1,0:T(8,128)} %get-tuple-element.52), channel_id=1, source_target_pairs={{0,4},{4,0},{8,12},{12,8},{16,20},{20,16},{24,28},{28,24},{1,5},{5... | collective-permute-start | bytes 786440 | tf_op jit(solution)/shard_map/ppermute | solution.py:539
  56.0 36.1 %collective-permute-start.19 = (f32[32,512]{1,0:T(8,128)}, f32[32,512]{1,0:T(8,128)S(1)}, u32[]{:S(2)}, u32[]{:S(2)}) collective-permute-start(f32[32,512]{1,0:T(8,128)} %get-tuple-element.56), channel_id=1, source_target_pairs={{0,24},{4,28},{8,16},{12,20},{16,8},{20,12},{24,0},{28,4},{1,25},{... | collective-permute-start | bytes 196616 | tf_op jit(solution)/shard_map/ppermute | solution.py:539
  59.6 32.5 %collective-permute-start.18 = (f32[32,512]{1,0:T(8,128)}, f32[32,512]{1,0:T(8,128)S(1)}, u32[]{:S(2)}, u32[]{:S(2)}) collective-permute-start(f32[32,512]{1,0:T(8,128)} %get-tuple-element.55), channel_id=1, source_target_pairs={{0,16},{4,20},{8,24},{12,28},{16,0},{20,4},{24,8},{28,12},{1,17},{... | collective-permute-start | bytes 196616 | tf_op jit(solution)/shard_map/ppermute | solution.py:539
  59.6 32.5 %collective-permute-start.17 = (f32[32,512]{1,0:T(8,128)}, f32[32,512]{1,0:T(8,128)S(1)}, u32[]{:S(2)}, u32[]{:S(2)}) collective-permute-start(f32[32,512]{1,0:T(8,128)} %get-tuple-element.54), channel_id=1, source_target_pairs={{0,8},{4,12},{8,0},{12,4},{16,24},{20,28},{24,16},{28,20},{1,9},{5... | collective-permute-start | bytes 196616 | tf_op jit(solution)/shard_map/ppermute | solution.py:539
  92.9 65.8 %collective-permute-start.20 = (f32[32,512]{1,0:T(8,128)}, f32[32,512]{1,0:T(8,128)S(1)}, u32[]{:S(2)}, u32[]{:S(2)}) collective-permute-start(f32[32,512]{1,0:T(8,128)} %get-tuple-element.62.refs_0_), channel_id=1, source_target_pairs={{0,8},{4,12},{8,0},{12,4},{16,24},{20,28},{24,16},{28,20},{1,9},{5... | collective-permute-start | bytes 196616 | tf_op jit(solution)/shard_map/ppermute | solution.py:539
  94.1 64.6 %collective-permute-start.21 = (f32[32,512]{1,0:T(8,128)}, f32[32,512]{1,0:T(8,128)S(1)}, u32[]{:S(2)}, u32[]{:S(2)}) collective-permute-start(f32[32,512]{1,0:T(8,128)} %get-tuple-element.62.refs_0_), channel_id=1, source_target_pairs={{0,16},{4,20},{8,24},{12,28},{16,0},{20,4},{24,8},{28,12},{1,17},{... | collective-permute-start | bytes 196616 | tf_op jit(solution)/shard_map/ppermute | solution.py:539
  97.0 61.7 %collective-permute-start.22 = (f32[32,512]{1,0:T(8,128)}, f32[32,512]{1,0:T(8,128)S(1)}, u32[]{:S(2)}, u32[]{:S(2)}) collective-permute-start(f32[32,512]{1,0:T(8,128)} %get-tuple-element.62.refs_0_), channel_id=1, source_target_pairs={{0,24},{4,28},{8,16},{12,20},{16,8},{20,12},{24,0},{28,4},{1,25},{... | collective-permute-start | bytes 196616 | tf_op jit(solution)/shard_map/ppermute | solution.py:539
  156.9 8.8 %collective-permute-start = (f32[128,512]{1,0:T(8,128)}, f32[128,512]{1,0:T(8,128)S(1)}, u32[]{:S(2)}, u32[]{:S(2)}) collective-permute-start(f32[128,512]{1,0:T(8,128)} %get-tuple-element.45), channel_id=1, source_target_pairs={{0,4},{4,0},{8,12},{12,8},{16,20},{20,16},{24,28},{28,24},{1,5},{5... | collective-permute-start | bytes 786440 | tf_op jit(solution)/shard_map/ppermute | solution.py:539
  157.3 27.6 %collective-permute-start.10 = (f32[512,256]{1,0:T(8,128)S(1)}, f32[512,256]{1,0:T(8,128)S(1)}, u32[]{:S(2)}, u32[]{:S(2)}) collective-permute-start(f32[512,256]{1,0:T(8,128)S(1)} %copy-done.7), channel_id=1, source_target_pairs={{0,16},{4,20},{8,24},{12,28},{16,0},{20,4},{24,8},{28,12},{1,17},{... | collective-permute-start | bytes 1572872 | tf_op jit(solution)/shard_map/ppermute | solution.py:539
  163.6 9.0 %collective-permute-start.24 = (f32[8,128]{1,0:T(8,128)S(1)}, f32[8,128]{1,0:T(8,128)S(1)}, u32[]{:S(2)}, u32[]{:S(2)}) collective-permute-start(f32[8,128]{1,0:T(8,128)S(1)} %add.77), channel_id=1, source_target_pairs={{0,2},{1,3},{2,0},{3,1},{4,6},{5,7},{6,4},{7,5},{8,10},{9,11},{10,... | collective-permute-start | bytes 12296 | tf_op jit(solution)/shard_map/ppermute | solution.py:539
  168.2 41.2 %collective-permute-start.3 = (f32[32,512]{1,0:T(8,128)}, f32[32,512]{1,0:T(8,128)S(1)}, u32[]{:S(2)}, u32[]{:S(2)}) collective-permute-start(f32[32,512]{1,0:T(8,128)} %get-tuple-element.49), channel_id=1, source_target_pairs={{0,24},{4,28},{8,16},{12,20},{16,8},{20,12},{24,0},{28,4},{1,25},{... | collective-permute-start | bytes 196616 | tf_op jit(solution)/shard_map/ppermute | solution.py:539
  170.6 39.5 %collective-permute-start.2 = (f32[32,512]{1,0:T(8,128)}, f32[32,512]{1,0:T(8,128)S(1)}, u32[]{:S(2)}, u32[]{:S(2)}) collective-permute-start(f32[32,512]{1,0:T(8,128)} %get-tuple-element.48), channel_id=1, source_target_pairs={{0,16},{4,20},{8,24},{12,28},{16,0},{20,4},{24,8},{28,12},{1,17},{... | collective-permute-start | bytes 196616 | tf_op jit(solution)/shard_map/ppermute | solution.py:539
  175.1 11.5 %collective-permute-start.26 = (f32[128,512]{1,0:T(8,128)S(1)}, f32[128,512]{1,0:T(8,128)S(1)}, u32[]{:S(2)}, u32[]{:S(2)}) collective-permute-start(f32[128,512]{1,0:T(8,128)S(1)} %pad_maximum_fusion.7.refs_0_), channel_id=1, source_target_pairs={{0,4},{4,0},{8,12},{12,8},{16,20},{20,16},{24,28},{28,24},{1,5},{5... | collective-permute-start | bytes 786440 | tf_op jit(solution)/shard_map/ppermute | solution.py:539
  185.0 18.1 %collective-permute-start.11 = (f32[2,256,256]{2,1,0:T(8,128)S(1)}, f32[2,256,256]{2,1,0:T(8,128)S(1)}, u32[]{:S(2)}, u32[]{:S(2)}) collective-permute-start(f32[2,256,256]{2,1,0:T(8,128)S(1)} %pad_maximum_fusion.2), channel_id=1, source_target_pairs={{0,4},{4,0},{8,12},{12,8},{16,20},{20,16},{24,28},{28,24},{1,5},{5... | collective-permute-start | bytes 1572872 | tf_op jit(solution)/shard_map/ppermute | solution.py:539
  190.0 13.0 %collective-permute-start.27 = (bf16[256,512]{1,0:T(8,128)(2,1)}, bf16[256,512]{1,0:T(8,128)(2,1)S(1)}, u32[]{:S(2)}, u32[]{:S(2)}) collective-permute-start(bf16[256,512]{1,0:T(8,128)(2,1)} %get-tuple-element.61), channel_id=1, source_target_pairs={{0,16},{4,20},{8,24},{12,28},{16,0},{20,4},{24,8},{28,12},{1,17},{... | collective-permute-start | bytes 786440 | tf_op jit(solution)/shard_map/ppermute | solution.py:539
  190.0 19.3 %collective-permute-start.13 = (f32[2,256,256]{2,1,0:T(8,128)S(1)}, f32[2,256,256]{2,1,0:T(8,128)S(1)}, u32[]{:S(2)}, u32[]{:S(2)}) collective-permute-start(f32[2,256,256]{2,1,0:T(8,128)S(1)} %pad_maximum_fusion.3), channel_id=1, source_target_pairs={{0,8},{4,12},{8,0},{12,4},{16,24},{20,28},{24,16},{28,20},{1,9},{5... | collective-permute-start | bytes 1572872 | tf_op jit(solution)/shard_map/ppermute | solution.py:539
  203.0 9.2 %collective-permute-start.1 = (f32[32,512]{1,0:T(8,128)S(1)}, f32[32,512]{1,0:T(8,128)S(1)}, u32[]{:S(2)}, u32[]{:S(2)}) collective-permute-start(f32[32,512]{1,0:T(8,128)S(1)} %copy-done.24), channel_id=1, source_target_pairs={{0,8},{4,12},{8,0},{12,4},{16,24},{20,28},{24,16},{28,20},{1,9},{5... | collective-permute-start | bytes 196616 | tf_op jit(solution)/shard_map/ppermute | solution.py:539
  203.1 9.8 %collective-permute-start.28 = (bf16[2,128,512]{2,1,0:T(8,128)(2,1)S(1)}, bf16[2,128,512]{2,1,0:T(8,128)(2,1)S(1)}, u32[]{:S(2)}, u32[]{:S(2)}) collective-permute-start(bf16[2,128,512]{2,1,0:T(8,128)(2,1)S(1)} %pad_maximum_fusion.8), channel_id=1, source_target_pairs={{0,4},{4,0},{8,12},{12,8},{16,20},{20,16},{24,28},{28,24},{1,5},{5... | collective-permute-start | bytes 786440 | tf_op jit(solution)/shard_map/ppermute | solution.py:539
  209.3 64.5 %collective-permute-start.12 = (f32[4,256,256]{2,1,0:T(8,128)S(1)}, f32[4,256,256]{2,1,0:T(8,128)}, u32[]{:S(2)}, u32[]{:S(2)}) collective-permute-start(f32[4,256,256]{2,1,0:T(8,128)S(1)} %pad_maximum_fusion.refs_0_), channel_id=1, source_target_pairs={{0,8},{4,12},{8,0},{12,4},{16,24},{20,28},{24,16},{28,20},{1,9},{5... | collective-permute-start | bytes 3145736 | tf_op jit(solution)/shard_map/ppermute | solution.py:539
  209.4 64.4 %collective-permute-start.14 = (f32[4,256,256]{2,1,0:T(8,128)S(1)}, f32[4,256,256]{2,1,0:T(8,128)}, u32[]{:S(2)}, u32[]{:S(2)}) collective-permute-start(f32[4,256,256]{2,1,0:T(8,128)S(1)} %pad_maximum_fusion.1.refs_2_), channel_id=1, source_target_pairs={{0,4},{4,0},{8,12},{12,8},{16,20},{20,16},{24,28},{28,24},{1,5},{5... | collective-permute-start | bytes 3145736 | tf_op jit(solution)/shard_map/ppermute | solution.py:539
  210.0 31.6 %collective-permute-start.30 = (bf16[2,128,512]{2,1,0:T(8,128)(2,1)S(1)}, bf16[2,128,512]{2,1,0:T(8,128)(2,1)S(1)}, u32[]{:S(2)}, u32[]{:S(2)}) collective-permute-start(bf16[2,128,512]{2,1,0:T(8,128)(2,1)S(1)} %pad_maximum_fusion.9), channel_id=1, source_target_pairs={{0,8},{4,12},{8,0},{12,4},{16,24},{20,28},{24,16},{28,20},{1,9},{5... | collective-permute-start | bytes 786440 | tf_op jit(solution)/shard_map/ppermute | solution.py:539
  212.8 30.2 %collective-permute-start.4 = (f32[32,512]{1,0:T(8,128)S(1)}, f32[32,512]{1,0:T(8,128)S(1)}, u32[]{:S(2)}, u32[]{:S(2)}) collective-permute-start(f32[32,512]{1,0:T(8,128)S(1)} %get-tuple-element.65.refs_0_), channel_id=1, source_target_pairs={{0,8},{4,12},{8,0},{12,4},{16,24},{20,28},{24,16},{28,20},{1,9},{5... | collective-permute-start | bytes 196616 | tf_op jit(solution)/shard_map/ppermute | solution.py:539
  212.9 56.1 %collective-permute-start.29 = (bf16[4,128,512]{2,1,0:T(8,128)(2,1)S(1)}, bf16[4,128,512]{2,1,0:T(8,128)(2,1)}, u32[]{:S(2)}, u32[]{:S(2)}) collective-permute-start(bf16[4,128,512]{2,1,0:T(8,128)(2,1)S(1)} %pad_maximum_fusion.4.refs_0_), channel_id=1, source_target_pairs={{0,8},{4,12},{8,0},{12,4},{16,24},{20,28},{24,16},{28,20},{1,9},{5... | collective-permute-start | bytes 1572872 | tf_op jit(solution)/shard_map/ppermute | solution.py:539
  241.7 27.4 %collective-permute-start.31 = (bf16[4,128,512]{2,1,0:T(8,128)(2,1)S(1)}, bf16[4,128,512]{2,1,0:T(8,128)(2,1)}, u32[]{:S(2)}, u32[]{:S(2)}) collective-permute-start(bf16[4,128,512]{2,1,0:T(8,128)(2,1)S(1)} %pad_maximum_fusion.5.refs_2_), channel_id=1, source_target_pairs={{0,4},{4,0},{8,12},{12,8},{16,20},{20,16},{24,28},{28,24},{1,5},{5... | collective-permute-start | bytes 1572872 | tf_op jit(solution)/shard_map/ppermute | solution.py:539
  (35 other events, 601.3 us)

commit v2 on v1

--- a/solution.py
+++ b/solution.py
@@ -22,6 +22,7 @@
 BF16 = jnp.bfloat16
 NT = (((1,), (1,)), ((), ()))
 VMEM_BYTES = 60 * 2**20
+KERNEL_BYTES = 24 * 2**20
 
 
 def split_pair(x):
@@ -39,25 +40,63 @@
             send_ref[p * rows : (p + 1) * rows, :] = proj_ref[pl.ds(at, rows), :]
 
 
-def value_proj_kernel(outer, place_ref, x_ref, c_ref, basis_ref, proj_ref, *send_refs):
+def in_hbm(x):
+    return pltpu.with_memory_space_constraint(x, pltpu.HBM)
+
+
+def fetch(step, last, copies):
+    @pl.when(step == 0)
+    def _():
+        for copy in copies():
+            copy.start()
+
+    def finish():
+        @pl.when(step == last)
+        def _():
+            for copy in copies():
+                copy.wait()
+
+    return finish
+
+
+def value_proj_kernel(
+    outer, place_ref, x_ref, c_ref, basis_ref, other_hbm, other_basis_hbm, proj_ref, *rest
+):
+    *send_refs, other_ref, other_basis_ref, sems = rest
+    step, last = pl.program_id(0), pl.num_programs(0) - 1
+
+    def copies():
+        pieces = sems.shape[0] - 1
+        rows = other_ref.shape[0] // pieces
+        return [
+            pltpu.make_async_copy(
+                other_hbm.at[pl.ds(i * rows, rows), :],
+                other_ref.at[pl.ds(i * rows, rows), :],
+                sems.at[i],
+            )
+            for i in range(pieces)
+        ] + [pltpu.make_async_copy(other_basis_hbm, other_basis_ref, sems.at[pieces])]
+
+    finish = fetch(step, last, copies)
     y = jnp.dot(x_ref[...], basis_ref[...], preferred_element_type=F32)
     high, low = split_pair(y.T)
     part = jnp.dot(high, c_ref[...], preferred_element_type=F32) + jnp.dot(
         low, c_ref[...], preferred_element_type=F32
     )
 
-    @pl.when(pl.program_id(0) == 0)
+    @pl.when(step == 0)
     def _():
         proj_ref[...] = part
 
-    @pl.when(pl.program_id(0) > 0)
+    @pl.when(step > 0)
     def _():
         proj_ref[...] += part
 
-
-    @pl.when(pl.program_id(0) == pl.num_programs(0) - 1)
+    @pl.when(step == last)
     def _():
         write_sends(place_ref, outer, proj_ref, send_refs)
+
+    finish()
 
 
 def sends_shape(rank, cols):
@@ -65,108 +104,123 @@
     return [jax.ShapeDtypeStruct((rank // inner, cols), F32)] * (inner - 1)
 
 
-def value_proj(place, x, c, basis):
+def value_proj(place, x, c, basis, other, other_basis):
     tokens, width = x.shape
     rank, cols = basis.shape[1], c.shape[1]
     block = min(512, tokens)
     outer, inner = groups_of("fs")
+    vmem = pl.BlockSpec(memory_space=pltpu.VMEM)
+    hbm = pl.BlockSpec(memory_space=pl.ANY)
     return pl.pallas_call(
         functools.partial(value_proj_kernel, outer),
         grid=(tokens // block,),
-        out_shape=[jax.ShapeDtypeStruct((rank, cols), F32)] + sends_shape(rank, cols),
+        out_shape=[jax.ShapeDtypeStruct((rank, cols), F32)]
+        + sends_shape(rank, cols)
+        + [pltpu.VMEM(other.shape, BF16), pltpu.VMEM(other_basis.shape, BF16)],
         in_specs=[
             pl.BlockSpec(memory_space=pltpu.SMEM),
             pl.BlockSpec((block, width), lambda t: (t, 0)),
             pl.BlockSpec((block, cols), lambda t: (t, 0)),
             pl.BlockSpec((width, rank), lambda t: (0, 0)),
+            hbm,
+            hbm,
         ],
         out_specs=[pl.BlockSpec((rank, cols), lambda t: (0, 0))]
-        + [pl.BlockSpec((rank // inner, cols), lambda t: (0, 0))] * (inner - 1),
+        + [pl.BlockSpec((rank // inner, cols), lambda t: (0, 0))] * (inner - 1)
+        + [vmem, vmem],
+        scratch_shapes=[pltpu.SemaphoreType.DMA((5,))],
         cost_estimate=pl.CostEstimate(
             flops=2 * tokens * rank * (width + 2 * cols),
-            bytes_accessed=2 * tokens * (width + cols),
+            bytes_accessed=2 * tokens * (2 * width + cols),
             transcendentals=0,
         ),
-        compiler_params=pltpu.CompilerParams(vmem_limit_bytes=VMEM_BYTES),
+        compiler_params=pltpu.CompilerParams(vmem_limit_bytes=KERNEL_BYTES),
         name="value_proj",
-    )(place, x, c, basis)
-
-
-def low_rank_kernel(x_ref, basis_ref, high_ref, low_ref):
-    y = jnp.dot(x_ref[...], basis_ref[...], preferred_element_type=F32)
-    high_ref[...], low_ref[...] = split_pair(y)
-
-
-def low_rank_rows(half, x, basis):
+    )(place, *map(in_hbm, (x, c, basis, other, other_basis)))
+
+
+def head_copies(sources, targets, sems, start):
+    count, _, width = targets[0].shape
+    return [
+        pltpu.make_async_copy(
+            source.at[:, pl.ds((start + j) * width, width)], target.at[j], sems.at[j, i]
+        )
+        for j in range(count)
+        for i, (source, target) in enumerate(zip(sources, targets))
+    ]
+
+
+def low_rank_kernel(half, start, x_ref, basis_ref, *refs):
+    if start is not None:
+        *sources, high_ref, low_ref, q_ref, k_ref, v_ref, sems = refs
+        copies = head_copies(sources, (q_ref, k_ref, v_ref), sems, start)
+        for copy in copies:
+            copy.start()
+    else:
+        copies = []
+        high_ref, low_ref = refs
+    rows = high_ref.shape[0]
+    few = min(512, rows)
+    for t in range(rows // few):
+        y = jnp.dot(
+            x_ref[half * rows + t * few : half * rows + (t + 1) * few, :],
+            basis_ref[...],
+            preferred_element_type=F32,
+        )
+        high, low = split_pair(y)
+        high_ref[t * few : (t + 1) * few, :] = high
+        low_ref[t * few : (t + 1) * few, :] = low
+    for copy in copies:
+        copy.wait()
+
+
+def heads_in_vmem(count, sources, heads):
+    return [
+        pltpu.VMEM((count, source.shape[0], source.shape[1] // heads), BF16)
+        for source in sources
+    ]
+
+
+def low_rank_rows(half, x, basis, sources, heads, span):
     tokens, width = x.shape[0] // 2, x.shape[1]
     rank = basis.shape[1]
-    block = min(512, tokens)
-    skip = half * (tokens // block)
-    out = jax.ShapeDtypeStruct((tokens, rank), BF16)
+    vmem = pl.BlockSpec(memory_space=pltpu.VMEM)
+    fetched = heads_in_vmem(span[1] - span[0], sources, heads) if span else []
+    sources = sources if span else []
     return pl.pallas_call(
-        low_rank_kernel,
-        grid=(tokens // block,),
-        out_shape=(out, out),
-        in_specs=[
-            pl.BlockSpec((block, width), lambda t: (t + skip, 0)),
-            pl.BlockSpec((width, rank), lambda t: (0, 0)),
-        ],
-        out_specs=[pl.BlockSpec((block, rank), lambda t: (t, 0))] * 2,
+        functools.partial(low_rank_kernel, half, span[0] if span else None),
+        out_shape=[pltpu.VMEM((tokens, rank), BF16)] * 2 + fetched,
+        in_specs=[vmem, vmem] + [pl.BlockSpec(memory_space=pl.ANY)] * len(sources),
+        out_specs=[vmem] * (2 + len(fetched)),
+        scratch_shapes=[pltpu.SemaphoreType.DMA((span[1] - span[0], 3))] if span else [],
         cost_estimate=pl.CostEstimate(
             flops=2 * tokens * rank * width,
             bytes_accessed=2 * tokens * width,
             transcendentals=0,
         ),
-        compiler_params=pltpu.CompilerParams(vmem_limit_bytes=VMEM_BYTES),
+        compiler_params=pltpu.CompilerParams(vmem_limit_bytes=KERNEL_BYTES),
         name="low_rank_rows",
-    )(x, basis)
+    )(x, basis, *map(in_hbm, sources))
 
 
 def attend_kernel(
-    bq, start, outer, inner, place_ref, lam_ref, gain_ref, q_hbm, k_hbm, v_hbm, high_hbm,
-    low_hbm, high_two, low_two, *rest
+    bq, start, outer, inner, after_start, place_ref, lam_ref, gain_ref, q_all, k_all, v_all,
+    high_one, low_one, high_two, low_two, *rest
 ):
-    q_all, k_all, v_all, high_ref, low_ref, e_ref, h_ref, sum_ref, sems, late_sems = rest[-10:]
-    proj_ref, *send_refs = rest[-10 - inner : -10]
-    count, seq, width = q_all.shape
-    step = pl.program_id(0)
-
-    def head_copies(j):
-        columns = pl.ds(pl.multiple_of((start + j) * width, width), width)
-        return [
-            pltpu.make_async_copy(source.at[:, columns], target.at[j], sems.at[j, i])
-            for i, (source, target) in enumerate(
-                ((k_hbm, k_all), (q_hbm, q_all), (v_hbm, v_all))
-            )
-        ]
-
-    def late_copies():
-        pairs = ((high_hbm, high_ref), (low_hbm, low_ref), (high_two, high_ref), (low_two, low_ref))
-        return [
-            pltpu.make_async_copy(
-                source,
-                target.at[pl.ds(i // 2 * (seq // 2), seq // 2), :],
-                late_sems.at[i],
-            )
-            for i, (source, target) in enumerate(pairs)
-        ]
-
-    @pl.when(step == 0)
-    def _():
-        for copy in head_copies(0):
-            copy.start()
-
-    for copy in head_copies(step):
-        copy.wait()
-
-    @pl.when(step == 0)
-    def _():
-        for copy in late_copies():
-            copy.start()
-        for j in range(1, count):
-            for copy in head_copies(j):
-                copy.start()
-
+    seq = q_all.shape[1]
+    width = q_all.shape[2]
+    step, last = pl.program_id(0), pl.num_programs(0) - 1
+    if after_start is None:
+        *rest, e_ref, h_ref, sum_ref = rest
+        finish_fetch = lambda: None
+    else:
+        sources, rest = rest[:3], rest[3:]
+        *rest, q_next, k_next, v_next, e_ref, h_ref, sum_ref, sems = rest
+        finish_fetch = fetch(
+            step, last,
+            lambda: head_copies(sources, (q_next, k_next, v_next), sems, after_start),
+        )
+    proj_ref, *send_refs = rest[-inner:]
     q_ref, k_ref, v_ref = q_all.at[step], k_all.at[step], v_all.at[step]
     half = width // 2
     lam = lam_ref[start + step]
@@ -244,73 +298,70 @@
 
         lax.fori_loop(0, seq // few, block, 0)
 
-    @pl.when(step == 0)
-    def _():
-        for copy in late_copies():
-            copy.wait()
-
-    h = h_ref[...]
-    turned = jnp.dot(h, high_ref[...], preferred_element_type=F32) + jnp.dot(
-        h, low_ref[...], preferred_element_type=F32
-    )
+    turned = jnp.zeros((h_ref.shape[0], high_one.shape[1]), F32)
+    for part, pair in enumerate(((high_one, low_one), (high_two, low_two))):
+        h = h_ref[:, part * (seq // 2) : (part + 1) * (seq // 2)]
+        for ref in pair:
+            turned = turned + jnp.dot(h, ref[...], preferred_element_type=F32)
     proj_ref[...] = turned.T
     write_sends(place_ref, outer, proj_ref, send_refs)
+    finish_fetch()
 
 
 def attend_heads(
-    start, stop, place, query_rows, key_rows, value_rows, mix_lambda, head_gain, pairs,
-    earlier,
+    span, after_span, place, held, sources, mix_lambda, head_gain, pairs, earlier
 ):
-    seq = query_rows.shape[0]
+    seq = sources[0].shape[0]
     heads = mix_lambda.shape[0]
+    start, stop = span
     count = stop - start
-    width = query_rows.shape[1] // heads
     rank = pairs[0][0].shape[1]
     bq = min(256, seq)
     outer, inner = groups_of("fs")
+    vmem = pl.BlockSpec(memory_space=pltpu.VMEM)
     hbm = pl.BlockSpec(memory_space=pl.ANY)
+    fetched, extra = [], []
+    if after_span:
+        ahead = after_span[1] - after_span[0]
+        fetched = heads_in_vmem(ahead, sources, heads)
+        extra = [pltpu.SemaphoreType.DMA((ahead, 3))]
+    sources = list(map(in_hbm, sources)) if after_span else []
     return pl.pallas_call(
-        functools.partial(attend_kernel, bq, start, outer, inner),
+        functools.partial(
+            attend_kernel, bq, start, outer, inner, after_span and after_span[0]
+        ),
         grid=(count,),
         out_shape=[jax.ShapeDtypeStruct((rank, heads * DV), F32)]
-        + sends_shape(rank, heads * DV),
-        in_specs=[
-            pl.BlockSpec(memory_space=pltpu.SMEM),
-            pl.BlockSpec(memory_space=pltpu.SMEM),
-            pl.BlockSpec(memory_space=pltpu.VMEM),
-        ]
-        + [hbm] * (7 + len(earlier)),
+        + sends_shape(rank, heads * DV)
+        + fetched,
+        in_specs=[pl.BlockSpec(memory_space=pltpu.SMEM)] * 2
+        + [vmem] * 8
+        + [hbm] * (len(sources) + len(earlier)),
         out_specs=[pl.BlockSpec((rank, DV), lambda j: (0, j + start))]
-        + [pl.BlockSpec((rank // inner, DV), lambda j: (0, j + start))] * (inner - 1),
-        input_output_aliases={10 + i: i for i in range(len(earlier))},
+        + [pl.BlockSpec((rank // inner, DV), lambda j: (0, j + start))] * (inner - 1)
+        + [vmem] * len(fetched),
+        input_output_aliases={10 + len(sources) + i: i for i in range(len(earlier))},
         scratch_shapes=[
-            pltpu.VMEM((count, seq, width), BF16),
-            pltpu.VMEM((count, seq, width), BF16),
-            pltpu.VMEM((count, seq, DV), BF16),
-            pltpu.VMEM((seq, rank), BF16),
-            pltpu.VMEM((seq, rank), BF16),
             pltpu.VMEM((2, 2 * bq, seq), F32),
             pltpu.VMEM((DV, seq), BF16),
             pltpu.VMEM((2, 2 * bq, 128), F32),
-            pltpu.SemaphoreType.DMA((count, 3)),
-            pltpu.SemaphoreType.DMA((4,)),
-        ],
+        ]
+        + extra,
         cost_estimate=pl.CostEstimate(
             flops=8 * count * seq * seq * DV,
-            bytes_accessed=2 * seq * (count * (2 * width + DV) + 2 * rank),
+            bytes_accessed=8 * seq * (count * DV + rank),
             transcendentals=count * seq * seq,
         ),
-        compiler_params=pltpu.CompilerParams(vmem_limit_bytes=VMEM_BYTES),
+        compiler_params=pltpu.CompilerParams(vmem_limit_bytes=KERNEL_BYTES),
         name="attend_heads",
     )(
         place,
         mix_lambda,
         head_gain.reshape(1, DV),
-        query_rows,
-        key_rows,
-        value_rows,
+        *held,
         *pairs[0],
         *pairs[1],
+        *sources,
         *earlier,
     )
 
@@ -442,14 +493,14 @@
             bytes_accessed=14 * old.size,
             transcendentals=0,
         ),
-        name="value_final",
+        compiler_params=pltpu.CompilerParams(vmem_limit_bytes=14 * 2**20),
+    name="value_final",
     )(me.reshape(1), squares, owners, basis, old, *direction)
 
 
-def fold(part, arrived, inner, width, outer, groups, rows):
+def fold(place, part, arrived, groups, rows):
     cols = part.shape[1]
     vmem = pl.BlockSpec(memory_space=pltpu.VMEM)
-    place = jnp.stack([inner, jnp.int32(width), outer]).astype(jnp.int32)
     return pl.pallas_call(
         functools.partial(fold_kernel, len(arrived)),
         out_shape=[jax.ShapeDtypeStruct((rows, cols), F32)] * groups,
@@ -458,6 +509,7 @@
         cost_estimate=pl.CostEstimate(
             flops=part.size, bytes_accessed=8 * part.size, transcendentals=0
         ),
+        compiler_params=pltpu.CompilerParams(vmem_limit_bytes=6 * 2**20),
         name="fold",
     )(place, part, *arrived)
 
@@ -502,6 +554,7 @@
             bytes_accessed=4 * len(parts) * parts[0].size,
             transcendentals=0,
         ),
+        compiler_params=pltpu.CompilerParams(vmem_limit_bytes=4 * 2**20),
         name="square_sums",
     )(*parts)
 
@@ -550,12 +603,11 @@
     return outer, n // outer
 
 
-def reduce_scatter(x, sends, axis):
+def reduce_scatter(place, x, sends, axis):
     outer, inner = groups_of(axis)
-    me = lax.axis_index(axis)
     rows = x.shape[0] // (outer * inner)
     arrived = [swap(send, axis, d) for d, send in enumerate(sends, 1)]
-    sums = fold(x, arrived, me % inner, inner, me // inner, outer, rows)
+    sums = fold(place, x, arrived, outer, rows)
     total = sums[0]
     for d in range(1, outer):
         total = total + swap(sums[d], axis, d * inner)
@@ -578,7 +630,7 @@
 
 def gather_by_distance(x, axis):
     bits = bits_down(lax.axis_size(axis))
-    other = swap(x, axis, bits[0])
+    x, other = lax.optimization_barrier((x, swap(x, axis, bits[0])))
     rows = x.shape[0] // 2
     parts, owners = [], []
     for g, order in enumerate((bits[:0:-1], bits[1:])):
@@ -628,9 +680,12 @@
     me = lax.axis_index("fs")
     parts, owners = gather_by_distance(out_weight, "fs")
 
-    place = (me % groups_of("fs")[1]).reshape(1)
-    value_part, *value_sends = value_proj(place, layer_input, value_cotangent, value_basis)
-    value_sum = reduce_scatter(value_part, value_sends, "fs")
+    inner = groups_of("fs")[1]
+    place = jnp.stack([me % inner, jnp.int32(inner), me // inner]).astype(jnp.int32)
+    value_part, *value_sends, cotangent, basis = value_proj(
+        place, layer_input, value_cotangent, value_basis, out_cotangent, out_basis
+    )
+    value_sum = reduce_scatter(place, value_part, value_sends, "fs")
     new_value_first, new_value_second, value_dir = moment_step(
         value_sum, value_first, value_second
     )
@@ -640,16 +695,21 @@
     )
     value_copy = assemble(owners, gather_by_distance(value_rounded, "fs")[0])
 
-    pairs = [low_rank_rows(half, out_cotangent, out_basis) for half in range(2)]
     heads = mix_lambda.shape[0]
-    out_parts = ()
+    sources = [query_rows, key_rows, value_rows]
     cuts = sorted({0, heads // 4, heads // 2, heads})
-    for start, stop in zip(cuts[:-1], cuts[1:]):
-        out_parts = attend_heads(
-            start, stop, place, query_rows, key_rows, value_rows, mix_lambda,
-            head_gain, pairs, out_parts,
+    spans = list(zip(cuts[:-1], cuts[1:])) + [None]
+    pair_one = low_rank_rows(0, cotangent, basis, sources, heads, None)
+    high, low, *held = low_rank_rows(1, cotangent, basis, sources, heads, spans[0])
+    out_parts = []
+    for call, span in enumerate(spans[:-1]):
+        outs = attend_heads(
+            span, spans[call + 1], place, held, sources, mix_lambda, head_gain,
+            (pair_one, (high, low)), out_parts,
         )
-    out_sum = reduce_scatter(out_parts[0], out_parts[1:], "fs")
+        inner = groups_of("fs")[1]
+        out_parts, held = list(outs[:inner]), outs[inner:]
+    out_sum = reduce_scatter(place, out_parts[0], out_parts[1:], "fs")
     new_out_first, new_out_second, out_dir = moment_step(out_sum, out_first, out_second)
     out_dirs, out_owners, *out_squares = gather_and_square(out_dir)
     out_copy, out_step, new_out_weight = out_final(

time: 281 us -> 254 us (0.904)
  Pallas kernels: 158 us -> 141 us
  starting transfers between devices: 37.4 us -> 42.7 us
  local copies, waits for them, and re-layouts: 5.85 us -> 0.97 us
  other arithmetic: 7.9 us -> 3.08 us
  waiting for transfers between devices: 69.2 us -> 65 us
    pallas_call x5, Pallas kernels: 131 us -> 119 us  [the longest x3 116 us: attend_heads(): pl.pallas_call(functools.partial(attend_kernel, bq, start, outer, inner,...]
    ppermute x32, starting transfers between devices: 37.4 us -> 42.7 us  [swap(): return lax.ppermute(x, axis, [(i, i ^ bit) for i in range(n)])]
    ppermute x32, waiting for transfers between devices: 69.2 us -> 65 us  [swap(): return lax.ppermute(x, axis, [(i, i ^ bit) for i in range(n)])]
    unnamed x54 -> x36, local copies, waits for them, and re-layouts: 4.78 us -> 0.86 us
    pallas_call x2, Pallas kernels: 3.09 us -> 0.05 us  [square_sums(): pl.pallas_call(square_kernel, out_shape=jax.ShapeDtypeStruct((8, 128), F3...]
  transfers between devices with their start and end apart: 32 -> 32, of which waited for: 13 -> 13; matrix products, arithmetic and copies ran while one was open for 3% -> 1% of each run, Pallas kernels for 51% -> 49%
where the time goes in v2:
time: 254 us
  Pallas kernels  141 us (56%)
  waiting for transfers between devices  65 us (26%)
  starting transfers between devices  42.7 us (17%)
  other arithmetic  3.08 us (1%)
    pallas_call x3, Pallas kernels, attend_heads(): pl.pallas_call(functools.partial(attend_kernel, bq, start, outer, inner,...  116 us
    ppermute x32, waiting for transfers between devices, swap(): return lax.ppermute(x, axis, [(i, i ^ bit) for i in range(n)])  65 us
    ppermute x32, starting transfers between devices, swap(): return lax.ppermute(x, axis, [(i, i ^ bit) for i in range(n)])  42.7 us
    pallas_call x1, Pallas kernels, value_proj(): pl.pallas_call(functools.partial(value_proj_kernel, outer), grid=(tokens...  10.1 us
    pallas_call x1, Pallas kernels, out_final(): pl.pallas_call(functools.partial(out_final_kernel, entries), out_shape=(j...  5.42 us
  transfers between devices with their start and end apart: 32, of which 13 were waited for; matrix products, arithmetic and copies ran while one was open for 1% of the time, Pallas kernels for 49%

profile of v2, /device:TPU:0, one launch (start us, length us, event | category | flops | bytes accessed | tf_op | source)
XLA Modules:
  0.0 254.2 jit_solution(1877218607315284039)
XLA Ops:
  0.7 10.1 %value_proj.1 = (f32[256,512]{1,0:T(8,128)S(1)}, f32[128,512]{1,0:T(8,128)S(1)}, bf16[2048,2048]{1,0:T(8,128)(2,1)S(1)}, bf16[2048,256]{1,0:T(8,128)(2,1)S(1)}) custom-call(s32[3]{0:T(128)S(1)} %pad_add_fusion.place_ref, bf16[2048,2048]{1,0:T(8,128)(2,1)} %x_ref.1, bf16[2048,512]{1,0:T(8,128)(2,1)} %c_ref.1, bf16[2048,256]{1,0:T(8,128)(2,1)} %basis_ref.5, ...), custom_call_target="tpu_custom_call" | custom-call | flops 3221225472 | bytes 18874368 | tf_op jit(solution)/shard_map/value_proj/pallas_call | solution.py:114
  10.9 3.0 %collective-permute-start.16 = (f32[128,512]{1,0:T(8,128)S(1)}, f32[128,512]{1,0:T(8,128)S(1)}, u32[]{:S(2)}, u32[]{:S(2)}) collective-permute-start(f32[128,512]{1,0:T(8,128)S(1)} %get-tuple-element.80), channel_id=1, source_target_pairs={{0,4},{4,0},{8,12},{12,8},{16,20},{20,16},{24,28},{28,24},{1,5},{5... | collective-permute-start | bytes 786440 | tf_op jit(solution)/shard_map/ppermute | solution.py:592
  13.9 2.6 %collective-permute-start.10 = (f32[512,256]{1,0:T(8,128)S(1)}, f32[512,256]{1,0:T(8,128)S(1)}, u32[]{:S(2)}, u32[]{:S(2)}) collective-permute-start(f32[512,256]{1,0:T(8,128)S(1)} %copy-done.11), channel_id=1, source_target_pairs={{0,16},{4,20},{8,24},{12,28},{16,0},{20,4},{24,8},{28,12},{1,17},{... | collective-permute-start | bytes 1572872 | tf_op jit(solution)/shard_map/ppermute | solution.py:592
  17.8 2.3 low_rank_rows.2
  20.8 3.9 %collective-permute-start.19 = (f32[32,512]{1,0:T(8,128)S(1)}, f32[32,512]{1,0:T(8,128)S(1)}, u32[]{:S(2)}, u32[]{:S(2)}) collective-permute-start(f32[32,512]{1,0:T(8,128)S(1)} %get-tuple-element.84), channel_id=1, source_target_pairs={{0,24},{4,28},{8,16},{12,20},{16,8},{20,12},{24,0},{28,4},{1,25},{... | collective-permute-start | bytes 196616 | tf_op jit(solution)/shard_map/ppermute | solution.py:592
  25.3 29.0 %attend_heads.3 = (f32[256,512]{1,0:T(8,128)S(1)}, f32[128,512]{1,0:T(8,128)S(1)}, bf16[1,2048,128]{2,1,0:T(8,128)(2,1)S(1)}, bf16[1,2048,128]{2,1,0:T(8,128)(2,1)S(1)}, bf16[1,2048,128]{2,1,0:T(8,128)(2,1)S(1)}) custom-call(s32[3]{0:T(128)S(1)} %pad_add_fusion.place_ref, f32[4]{0:T(128)S(1)} %copy-done.3, f32[1,128]{1,0:T(1,128)S(1)} %bitcast.20, ...), custom_call_target="tpu_custom_call" | custom-call | flops 4294967296 | bytes 6291456 | tf_op jit(solution)/shard_map/attend_heads/pallas_call | solution.py:329
  56.5 2.9 %collective-permute-start.21 = (f32[32,512]{1,0:T(8,128)S(1)}, f32[32,512]{1,0:T(8,128)S(1)}, u32[]{:S(2)}, u32[]{:S(2)}) collective-permute-start(f32[32,512]{1,0:T(8,128)S(1)} %get-tuple-element.92.refs_0_), channel_id=1, source_target_pairs={{0,16},{4,20},{8,24},{12,28},{16,0},{20,4},{24,8},{28,12},{1,17},{... | collective-permute-start | bytes 196616 | tf_op jit(solution)/shard_map/ppermute | solution.py:592
  59.5 29.0 %attend_heads.4 = (f32[256,512]{1,0:T(8,128)S(1)}, f32[128,512]{1,0:T(8,128)S(1)}, bf16[2,2048,128]{2,1,0:T(8,128)(2,1)S(1)}, bf16[2,2048,128]{2,1,0:T(8,128)(2,1)S(1)}, bf16[2,2048,128]{2,1,0:T(8,128)(2,1)S(1)}) custom-call(s32[3]{0:T(128)S(1)} %pad_add_fusion.place_ref, f32[4]{0:T(128)S(1)} %copy-done.3, ...), custom_call_target="tpu_custom_call", output_to_operand_aliasing={{0}: (13, {}), {1}: (14, {})} | custom-call | flops 4294967296 | bytes 6291456 | tf_op jit(solution)/shard_map/attend_heads/pallas_call | solution.py:329
  88.6 57.9 %attend_heads.5 = (f32[256,512]{1,0:T(8,128)S(1)}, f32[128,512]{1,0:T(8,128)S(1)}) custom-call(s32[3]{0:T(128)S(1)} %pad_add_fusion.place_ref, f32[4]{0:T(128)S(1)} %copy-done.3, f32[1,128]{1,0:T(1,128)S(1)} %bitcast.22, bf16[2,2048,128]{2,1,0:T(8,128)(2,1)S(1)} %get-tuple-element.65.q_all, ...), custom_call_target="tpu_custom_call", output_to_operand_aliasing={{0}: (10, {}), {1}: (11, {})} | custom-call | flops 8589934592 | bytes 8388608 | tf_op jit(solution)/shard_map/attend_heads/pallas_call | solution.py:329
  149.8 2.1 collective-permute-done.24
  155.9 4.8 %collective-permute-done.26.refs_1_ = f32[128,512]{1,0:T(8,128)S(1)} collective-permute-done((f32[128,512]{1,0:T(8,128)S(1)}, f32[128,512]{1,0:T(8,128)S(1)}, u32[]{:S(2)}, u32[]{:S(2)}) %collective-permute-start.26) | collective-permute-done | bytes 262176 | tf_op jit(solution)/shard_map/ppermute | solution.py:592
  165.7 3.0 %collective-permute-start.13 = (f32[2,256,256]{2,1,0:T(8,128)S(1)}, f32[2,256,256]{2,1,0:T(8,128)S(1)}, u32[]{:S(2)}, u32[]{:S(2)}) collective-permute-start(f32[2,256,256]{2,1,0:T(8,128)S(1)} %pad_maximum_fusion.3), channel_id=1, source_target_pairs={{0,8},{4,12},{8,0},{12,4},{16,24},{20,28},{24,16},{28,20},{1,9},{5... | collective-permute-start | bytes 1572872 | tf_op jit(solution)/shard_map/ppermute | solution.py:592
  170.8 7.2 %collective-permute-done.27 = bf16[256,512]{1,0:T(8,128)(2,1)S(1)} collective-permute-done((bf16[256,512]{1,0:T(8,128)(2,1)S(1)}, bf16[256,512]{1,0:T(8,128)(2,1)S(1)}, u32[]{:S(2)}, u32[]{:S(2)}) %collective-permute-start.27) | collective-permute-done | bytes 262176 | tf_op jit(solution)/shard_map/ppermute | solution.py:592
  179.7 8.3 %collective-permute-done.13 = f32[2,256,256]{2,1,0:T(8,128)S(1)} collective-permute-done((f32[2,256,256]{2,1,0:T(8,128)S(1)}, f32[2,256,256]{2,1,0:T(8,128)S(1)}, u32[]{:S(2)}, u32[]{:S(2)}) %collective-permute-start.13) | collective-permute-done | bytes 524320 | tf_op jit(solution)/shard_map/ppermute | solution.py:592
  189.0 2.1 collective-permute-start.30
  191.9 2.1 collective-permute-start.29
  194.0 26.4 %collective-permute-done.30 = bf16[2,128,512]{2,1,0:T(8,128)(2,1)S(1)} collective-permute-done((bf16[2,128,512]{2,1,0:T(8,128)(2,1)S(1)}, bf16[2,128,512]{2,1,0:T(8,128)(2,1)S(1)}, u32[]{:S(2)}, u32[]{:S(2)}) %collective-permute-start.30) | collective-permute-done | bytes 262176 | tf_op jit(solution)/shard_map/ppermute | solution.py:592
  222.0 5.5 %collective-permute-done.5.refs_2_ = f32[32,512]{1,0:T(8,128)S(1)} collective-permute-done((f32[32,512]{1,0:T(8,128)S(1)}, f32[32,512]{1,0:T(8,128)S(1)}, u32[]{:S(2)}, u32[]{:S(2)}) %collective-permute-start.5) | collective-permute-done | bytes 65568 | tf_op jit(solution)/shard_map/ppermute | solution.py:592
  227.5 3.2 %collective-permute-start.6 = (f32[32,512]{1,0:T(8,128)S(1)}, f32[32,512]{1,0:T(8,128)S(1)}, u32[]{:S(2)}, u32[]{:S(2)}) collective-permute-start(f32[32,512]{1,0:T(8,128)S(1)} %get-tuple-element.95.refs_0_), channel_id=1, source_target_pairs={{0,24},{4,28},{8,16},{12,20},{16,8},{20,12},{24,0},{28,4},{1,25},{... | collective-permute-start | bytes 196616 | tf_op jit(solution)/shard_map/ppermute | solution.py:592
  230.7 2.9 %collective-permute-done.6.refs_3_ = f32[32,512]{1,0:T(8,128)S(1)} collective-permute-done((f32[32,512]{1,0:T(8,128)S(1)}, f32[32,512]{1,0:T(8,128)S(1)}, u32[]{:S(2)}, u32[]{:S(2)}) %collective-permute-start.6) | collective-permute-done | bytes 65568 | tf_op jit(solution)/shard_map/ppermute | solution.py:592
  236.4 2.0 collective-permute-done.8
  239.9 2.1 collective-permute-done.9
  245.4 3.1 %assemble.1 = bf16[2048,512]{1,0:T(8,128)(2,1)} custom-call(s32[16]{0:T(128)} %broadcast_xor_fusion.1.owner_ref, bf16[4,128,512]{2,1,0:T(8,128)(2,1)} %copy-done.7, bf16[4,128,512]{2,1,0:T(8,128)(2,1)} %copy-done.10, bf16[4,128,512]{2,1,0:T(8,128)(2,1)} %copy-done.8, bf16[4,128,512]{2,1,0:T(8,128)(2,1)} %collective-permute-done.31.refs_3_), custom_call_target="tpu_custom_call" | custom-call | bytes 4194304 | tf_op jit(solution)/shard_map/assemble/pallas_call | solution.py:577
  248.6 5.4 %out_final.1 = (bf16[512,2048]{1,0:T(8,128)(2,1)}, f32[512,256]{1,0:T(8,128)}, f32[512,256]{1,0:T(8,128)}) custom-call(s32[16]{0:T(128)} %broadcast_xor_fusion.1.owner_ref, f32[8,128]{1,0:T(8,128)} %add.68.sum_ref, s32[8]{0:T(128)} %copy-done.2, bf16[2048,256]{1,0:T(8,128)(2,1)} %basis_ref.4, f32[4,256,256]{2,1,0:T(8,128)} %copy-done.5, ...), custom_call_target="tpu_custom_call" | custom-call | flops 1073741824 | bytes 6291456 | tf_op jit(solution)/shard_map/out_final/pallas_call | solution.py:413
  (112 shorter events, 32.0 us)
Async XLA Ops:
  10.9 9.3 %collective-permute-start.16 = (f32[128,512]{1,0:T(8,128)S(1)}, f32[128,512]{1,0:T(8,128)S(1)}, u32[]{:S(2)}, u32[]{:S(2)}) collective-permute-start(f32[128,512]{1,0:T(8,128)S(1)} %get-tuple-element.80), channel_id=1, source_target_pairs={{0,4},{4,0},{8,12},{12,8},{16,20},{20,16},{24,28},{28,24},{1,5},{5... | collective-permute-start | bytes 786440 | tf_op jit(solution)/shard_map/ppermute | solution.py:592
  13.9 142.0 %collective-permute-start.10 = (f32[512,256]{1,0:T(8,128)S(1)}, f32[512,256]{1,0:T(8,128)S(1)}, u32[]{:S(2)}, u32[]{:S(2)}) collective-permute-start(f32[512,256]{1,0:T(8,128)S(1)} %copy-done.11), channel_id=1, source_target_pairs={{0,16},{4,20},{8,24},{12,28},{16,0},{20,4},{24,8},{28,12},{1,17},{... | collective-permute-start | bytes 1572872 | tf_op jit(solution)/shard_map/ppermute | solution.py:592
  20.8 33.6 %collective-permute-start.19 = (f32[32,512]{1,0:T(8,128)S(1)}, f32[32,512]{1,0:T(8,128)S(1)}, u32[]{:S(2)}, u32[]{:S(2)}) collective-permute-start(f32[32,512]{1,0:T(8,128)S(1)} %get-tuple-element.84), channel_id=1, source_target_pairs={{0,24},{4,28},{8,16},{12,20},{16,8},{20,12},{24,0},{28,4},{1,25},{... | collective-permute-start | bytes 196616 | tf_op jit(solution)/shard_map/ppermute | solution.py:592
  24.7 29.7 %collective-permute-start.18 = (f32[32,512]{1,0:T(8,128)S(1)}, f32[32,512]{1,0:T(8,128)S(1)}, u32[]{:S(2)}, u32[]{:S(2)}) collective-permute-start(f32[32,512]{1,0:T(8,128)S(1)} %get-tuple-element.83), channel_id=1, source_target_pairs={{0,16},{4,20},{8,24},{12,28},{16,0},{20,4},{24,8},{28,12},{1,17},{... | collective-permute-start | bytes 196616 | tf_op jit(solution)/shard_map/ppermute | solution.py:592
  24.7 29.7 %collective-permute-start.17 = (f32[32,512]{1,0:T(8,128)S(1)}, f32[32,512]{1,0:T(8,128)S(1)}, u32[]{:S(2)}, u32[]{:S(2)}) collective-permute-start(f32[32,512]{1,0:T(8,128)S(1)} %get-tuple-element.82), channel_id=1, source_target_pairs={{0,8},{4,12},{8,0},{12,4},{16,24},{20,28},{24,16},{28,20},{1,9},{5... | collective-permute-start | bytes 196616 | tf_op jit(solution)/shard_map/ppermute | solution.py:592
  55.1 33.4 %collective-permute-start.20 = (f32[32,512]{1,0:T(8,128)S(1)}, f32[32,512]{1,0:T(8,128)S(1)}, u32[]{:S(2)}, u32[]{:S(2)}) collective-permute-start(f32[32,512]{1,0:T(8,128)S(1)} %get-tuple-element.92.refs_0_), channel_id=1, source_target_pairs={{0,8},{4,12},{8,0},{12,4},{16,24},{20,28},{24,16},{28,20},{1,9},{5... | collective-permute-start | bytes 196616 | tf_op jit(solution)/shard_map/ppermute | solution.py:592
  56.5 32.0 %collective-permute-start.21 = (f32[32,512]{1,0:T(8,128)S(1)}, f32[32,512]{1,0:T(8,128)S(1)}, u32[]{:S(2)}, u32[]{:S(2)}) collective-permute-start(f32[32,512]{1,0:T(8,128)S(1)} %get-tuple-element.92.refs_0_), channel_id=1, source_target_pairs={{0,16},{4,20},{8,24},{12,28},{16,0},{20,4},{24,8},{28,12},{1,17},{... | collective-permute-start | bytes 196616 | tf_op jit(solution)/shard_map/ppermute | solution.py:592
  59.4 29.1 %collective-permute-start.22 = (f32[32,512]{1,0:T(8,128)S(1)}, f32[32,512]{1,0:T(8,128)S(1)}, u32[]{:S(2)}, u32[]{:S(2)}) collective-permute-start(f32[32,512]{1,0:T(8,128)S(1)} %get-tuple-element.92.refs_0_), channel_id=1, source_target_pairs={{0,24},{4,28},{8,16},{12,20},{16,8},{20,12},{24,0},{28,4},{1,25},{... | collective-permute-start | bytes 196616 | tf_op jit(solution)/shard_map/ppermute | solution.py:592
  88.5 59.7 %collective-permute-start.23 = (f32[8,128]{1,0:T(8,128)S(1)}, f32[8,128]{1,0:T(8,128)S(1)}, u32[]{:S(2)}, u32[]{:S(2)}) collective-permute-start(f32[8,128]{1,0:T(8,128)S(1)} %square_sums.3), channel_id=1, source_target_pairs={{0,1},{1,0},{2,3},{3,2},{4,5},{5,4},{6,7},{7,6},{8,9},{9,8},{10,11... | collective-permute-start | bytes 12296 | tf_op jit(solution)/shard_map/ppermute | solution.py:592
  146.5 22.1 %collective-permute-start = (f32[128,512]{1,0:T(8,128)S(1)}, f32[128,512]{1,0:T(8,128)S(1)}, u32[]{:S(2)}, u32[]{:S(2)}) collective-permute-start(f32[128,512]{1,0:T(8,128)S(1)} %get-tuple-element.71), channel_id=1, source_target_pairs={{0,4},{4,0},{8,12},{12,8},{16,20},{20,16},{24,28},{28,24},{1,5},{5... | collective-permute-start | bytes 786440 | tf_op jit(solution)/shard_map/ppermute | solution.py:592
  152.3 8.5 %collective-permute-start.26 = (f32[128,512]{1,0:T(8,128)S(1)}, f32[128,512]{1,0:T(8,128)S(1)}, u32[]{:S(2)}, u32[]{:S(2)}) collective-permute-start(f32[128,512]{1,0:T(8,128)S(1)} %pad_maximum_fusion.7.refs_0_), channel_id=1, source_target_pairs={{0,4},{4,0},{8,12},{12,8},{16,20},{20,16},{24,28},{28,24},{1,5},{5... | collective-permute-start | bytes 786440 | tf_op jit(solution)/shard_map/ppermute | solution.py:592
  162.7 15.3 %collective-permute-start.27 = (bf16[256,512]{1,0:T(8,128)(2,1)S(1)}, bf16[256,512]{1,0:T(8,128)(2,1)S(1)}, u32[]{:S(2)}, u32[]{:S(2)}) collective-permute-start(bf16[256,512]{1,0:T(8,128)(2,1)S(1)} %get-tuple-element.90), channel_id=1, source_target_pairs={{0,16},{4,20},{8,24},{12,28},{16,0},{20,4},{24,8},{28,12},{1,17},{... | collective-permute-start | bytes 786440 | tf_op jit(solution)/shard_map/ppermute | solution.py:592
  164.1 14.0 %collective-permute-start.11 = (f32[2,256,256]{2,1,0:T(8,128)S(1)}, f32[2,256,256]{2,1,0:T(8,128)S(1)}, u32[]{:S(2)}, u32[]{:S(2)}) collective-permute-start(f32[2,256,256]{2,1,0:T(8,128)S(1)} %pad_maximum_fusion.2), channel_id=1, source_target_pairs={{0,4},{4,0},{8,12},{12,8},{16,20},{20,16},{24,28},{28,24},{1,5},{5... | collective-permute-start | bytes 1572872 | tf_op jit(solution)/shard_map/ppermute | solution.py:592
  165.7 22.4 %collective-permute-start.13 = (f32[2,256,256]{2,1,0:T(8,128)S(1)}, f32[2,256,256]{2,1,0:T(8,128)S(1)}, u32[]{:S(2)}, u32[]{:S(2)}) collective-permute-start(f32[2,256,256]{2,1,0:T(8,128)S(1)} %pad_maximum_fusion.3), channel_id=1, source_target_pairs={{0,8},{4,12},{8,0},{12,4},{16,24},{20,28},{24,16},{28,20},{1,9},{5... | collective-permute-start | bytes 1572872 | tf_op jit(solution)/shard_map/ppermute | solution.py:592
  169.2 18.9 %collective-permute-start.3 = (f32[32,512]{1,0:T(8,128)S(1)}, f32[32,512]{1,0:T(8,128)S(1)}, u32[]{:S(2)}, u32[]{:S(2)}) collective-permute-start(f32[32,512]{1,0:T(8,128)S(1)} %get-tuple-element.75), channel_id=1, source_target_pairs={{0,24},{4,28},{8,16},{12,20},{16,8},{20,12},{24,0},{28,4},{1,25},{... | collective-permute-start | bytes 196616 | tf_op jit(solution)/shard_map/ppermute | solution.py:592
  169.5 19.5 %collective-permute-start.2 = (f32[32,512]{1,0:T(8,128)S(1)}, f32[32,512]{1,0:T(8,128)S(1)}, u32[]{:S(2)}, u32[]{:S(2)}) collective-permute-start(f32[32,512]{1,0:T(8,128)S(1)} %get-tuple-element.74), channel_id=1, source_target_pairs={{0,16},{4,20},{8,24},{12,28},{16,0},{20,4},{24,8},{28,12},{1,17},{... | collective-permute-start | bytes 196616 | tf_op jit(solution)/shard_map/ppermute | solution.py:592
  178.0 13.1 %collective-permute-start.1 = (f32[32,512]{1,0:T(8,128)S(1)}, f32[32,512]{1,0:T(8,128)S(1)}, u32[]{:S(2)}, u32[]{:S(2)}) collective-permute-start(f32[32,512]{1,0:T(8,128)S(1)} %get-tuple-element.73), channel_id=1, source_target_pairs={{0,8},{4,12},{8,0},{12,4},{16,24},{20,28},{24,16},{28,20},{1,9},{5... | collective-permute-start | bytes 196616 | tf_op jit(solution)/shard_map/ppermute | solution.py:592
  178.1 13.8 %collective-permute-start.28 = (bf16[2,128,512]{2,1,0:T(8,128)(2,1)S(1)}, bf16[2,128,512]{2,1,0:T(8,128)(2,1)S(1)}, u32[]{:S(2)}, u32[]{:S(2)}) collective-permute-start(bf16[2,128,512]{2,1,0:T(8,128)(2,1)S(1)} %pad_maximum_fusion.8), channel_id=1, source_target_pairs={{0,4},{4,0},{8,12},{12,8},{16,20},{20,16},{24,28},{28,24},{1,5},{5... | collective-permute-start | bytes 786440 | tf_op jit(solution)/shard_map/ppermute | solution.py:592
  188.0 60.5 %collective-permute-start.12 = (f32[4,256,256]{2,1,0:T(8,128)S(1)}, f32[4,256,256]{2,1,0:T(8,128)}, u32[]{:S(2)}, u32[]{:S(2)}) collective-permute-start(f32[4,256,256]{2,1,0:T(8,128)S(1)} %pad_maximum_fusion.refs_0_), channel_id=1, source_target_pairs={{0,8},{4,12},{8,0},{12,4},{16,24},{20,28},{24,16},{28,20},{1,9},{5... | collective-permute-start | bytes 3145736 | tf_op jit(solution)/shard_map/ppermute | solution.py:592
  188.2 60.4 %collective-permute-start.14 = (f32[4,256,256]{2,1,0:T(8,128)S(1)}, f32[4,256,256]{2,1,0:T(8,128)}, u32[]{:S(2)}, u32[]{:S(2)}) collective-permute-start(f32[4,256,256]{2,1,0:T(8,128)S(1)} %pad_maximum_fusion.1.refs_2_), channel_id=1, source_target_pairs={{0,4},{4,0},{8,12},{12,8},{16,20},{20,16},{24,28},{28,24},{1,5},{5... | collective-permute-start | bytes 3145736 | tf_op jit(solution)/shard_map/ppermute | solution.py:592
  189.0 31.4 %collective-permute-start.30 = (bf16[2,128,512]{2,1,0:T(8,128)(2,1)S(1)}, bf16[2,128,512]{2,1,0:T(8,128)(2,1)S(1)}, u32[]{:S(2)}, u32[]{:S(2)}) collective-permute-start(bf16[2,128,512]{2,1,0:T(8,128)(2,1)S(1)} %pad_maximum_fusion.9), channel_id=1, source_target_pairs={{0,8},{4,12},{8,0},{12,4},{16,24},{20,28},{24,16},{28,20},{1,9},{5... | collective-permute-start | bytes 786440 | tf_op jit(solution)/shard_map/ppermute | solution.py:592
  191.8 30.0 %collective-permute-start.4 = (f32[32,512]{1,0:T(8,128)S(1)}, f32[32,512]{1,0:T(8,128)S(1)}, u32[]{:S(2)}, u32[]{:S(2)}) collective-permute-start(f32[32,512]{1,0:T(8,128)S(1)} %get-tuple-element.95.refs_0_), channel_id=1, source_target_pairs={{0,8},{4,12},{8,0},{12,4},{16,24},{20,28},{24,16},{28,20},{1,9},{5... | collective-permute-start | bytes 196616 | tf_op jit(solution)/shard_map/ppermute | solution.py:592
  191.9 52.7 %collective-permute-start.29 = (bf16[4,128,512]{2,1,0:T(8,128)(2,1)S(1)}, bf16[4,128,512]{2,1,0:T(8,128)(2,1)S(1)}, u32[]{:S(2)}, u32[]{:S(2)}) collective-permute-start(bf16[4,128,512]{2,1,0:T(8,128)(2,1)S(1)} %pad_maximum_fusion.4.refs_0_), channel_id=1, source_target_pairs={{0,8},{4,12},{8,0},{12,4},{16,24},{20,28},{24,16},{28,20},{1,9},{5... | collective-permute-start | bytes 1572872 | tf_op jit(solution)/shard_map/ppermute | solution.py:592
  220.5 24.2 %collective-permute-start.31 = (bf16[4,128,512]{2,1,0:T(8,128)(2,1)S(1)}, bf16[4,128,512]{2,1,0:T(8,128)(2,1)}, u32[]{:S(2)}, u32[]{:S(2)}) collective-permute-start(bf16[4,128,512]{2,1,0:T(8,128)(2,1)S(1)} %pad_maximum_fusion.5.refs_2_), channel_id=1, source_target_pairs={{0,4},{4,0},{8,12},{12,8},{16,20},{20,16},{24,28},{28,24},{1,5},{5... | collective-permute-start | bytes 1572872 | tf_op jit(solution)/shard_map/ppermute | solution.py:592
  (26 other events, 463.6 us)
